TPU v7x, 128 devices: a whole 4x4x4 slice. The times are simulated.
128 devices in a mesh: fs: 16 (over z, y), tp: 8 (over x, core).
Axes of the slice: x: 4, y: 4, z: 4, core: 2. Of those that a mesh axis runs over, the one named last changes fastest.
Arguments:
- tokens: bfloat16 [32768, 2048], P('fs'), may hold values from -6 to 6
- norm_gain: float32 [2048], replicated, may hold values from 0.1 to 1.9
- gate_weight: bfloat16 [2048, 5632], P('fs', 'tp'), may hold values from -0.125 to 0.125
- up_weight: bfloat16 [2048, 5632], P('fs', 'tp'), may hold values from -0.125 to 0.125
- down_weight: bfloat16 [5632, 2048], P('tp', 'fs'), may hold values from -0.078125 to 0.078125
Outputs:
- mixed: bfloat16 [32768, 2048], P(('fs', 'tp'))
All inputs are finite; a program needn't handle non-finite values.
Results may differ from a plain program's by a relative error of at most 0.014.
Values may be sent and summed in bfloat16 or wider, within the bound.
No kernel may reach another device: no remote copies, remote signals or barrier semaphores. Data moves between devices by JAX's collectives and lax.ppermute only.
A program may use at most 128 MiB of HBM per device.

v0:
```python
import jax
import jax.numpy as jnp
from jax import lax
from jax.sharding import PartitionSpec as P


def side_by_side(arrays, axis, dim, along):
    widths = [a.shape[along] for a in arrays]
    both = jnp.concatenate(arrays, axis=along)
    whole = lax.all_gather(both, axis, axis=dim, tiled=True)
    return tuple(jnp.split(whole, [sum(widths[:k]) for k in range(1, len(widths))], axis=along))


def from_everyone(value, axis):
    copies = jnp.broadcast_to(value, (lax.axis_size(axis), *value.shape))
    return lax.all_to_all(copies, axis, split_axis=0, concat_axis=0, tiled=True)


def laid_out(blocks, dim):
    shape = list(blocks.shape[1:])
    shape[dim] *= blocks.shape[0]
    return jnp.moveaxis(blocks, 0, dim).reshape(shape)


def gathered_copies(value, axis, dim):
    blocks = from_everyone(value, axis)
    return laid_out(blocks, dim)


def per_device(tokens, norm_gain, gate_weight, up_weight, down_weight):
    xf = tokens.astype(jnp.float32)
    scale = lax.rsqrt(jnp.mean(xf * xf, axis=-1, keepdims=True) + 1e-06)
    normed = (xf * scale * norm_gain).astype(jnp.bfloat16)
    gate_full, up_full = side_by_side((gate_weight, up_weight), "fs", 0, 1)
    gate = jnp.dot(normed, gate_full, preferred_element_type=jnp.float32)
    up = jnp.dot(normed, up_full, preferred_element_type=jnp.float32)
    hidden = (jax.nn.silu(gate) * up).astype(jnp.bfloat16)
    down_full = gathered_copies(down_weight, "fs", 1)
    return lax.psum_scatter(
        jnp.dot(hidden, down_full, preferred_element_type=jnp.float32).astype(jnp.bfloat16),
        "tp",
        scatter_dimension=0,
        tiled=True,
    )


def solution(mesh):
    placed = (P("fs", None), P(), P("fs", "tp"), P("fs", "tp"), P("tp", "fs"))
    return jax.shard_map(
        per_device, mesh=mesh, in_specs=placed, out_specs=P(("fs", "tp"), None), check_vma=False
    )
```

profile of v0, /device:TPU:1, one launch (start us, length us, event | category | flops | bytes accessed | tf_op | source)
XLA Modules:
  0.0 192.2 jit_solution(17103997552498888308)
XLA Ops:
  6.5 0.0 all-gather.2.cloned.1.call-start
  6.5 1.8 pad_maximum_fusion
  8.3 0.0 all-gather.2.cloned.1.call-update
  8.3 3.1 %broadcast_in_dim.2 = bf16[16,704,128]{2,1,0:T(8,128)(2,1)} broadcast(bf16[704,128]{1,0:T(8,128)(2,1)} %param.9), dimensions={1,2} | broadcast | bytes 3063808 | tf_op jit(solution)/shard_map/broadcast_in_dim | solution.py:15
  11.4 0.0 copy-start
  11.4 8.7 %all-to-all-start = ((bf16[16,704,128]{2,1,0:T(8,128)(2,1)}), bf16[16,704,128]{2,1,0:T(8,128)(2,1)S(1)}, u32[]{:S(2)}, u32[]{:S(2)}) async-start(bf16[16,704,128]{2,1,0:T(8,128)(2,1)} %broadcast_in_dim.2), calls=%async_computation | async-start | bytes 5767168 | tf_op jit(solution)/shard_map/all_to_all | solution.py:16
  20.1 0.0 reduce-scatter.2.cloned.1.call-start
  20.2 5.3 %fusion = f32[2048]{0:T(1024)S(1)} fusion(bf16[2048,2048]{1,0:T(8,128)(2,1)} %param.5), kind=kLoop, calls=%fused_computation.2 | loop fusion | flops 12580864 | bytes 8396800 | tf_op jit(solution)/shard_map/reduce_sum | solution.py:32
  25.5 76.7 %all-gather.2.cloned.1.call-done = bf16[2048,1408]{0,1:T(8,128)(2,1)} async-done(((bf16[128,1408]{0,1:T(8,128)(2,1)}), bf16[2048,1408]{0,1:T(8,128)(2,1)}) %all-gather.2.cloned.1.call-update) | async-done | bytes 5767184 | tf_op jit(solution)/shard_map/all_gather | solution.py:10
  102.2 0.0 copy-done
  102.2 11.2 %fusion.7 = f32[2048,704]{0,1:T(8,128)} fusion(bf16[2048,1408]{0,1:T(8,128)(2,1)} %all-gather.2.cloned.1.call-done, bf16[2048,2048]{1,0:T(8,128)(2,1)} %param.5, f32[2048]{0:T(1024)S(1)} %copy-done, f32[2048]{0:T(1024)S(1)} %add_rsqrt_fusion), kind=kOutput, calls=%fused_computation.10 | convolution fusion | flops 5922357248 | bytes 17055744 | tf_op jit(solution)/shard_map/dot_general | solution.py:35
  113.4 0.0 all-to-all-done
  113.4 19.3 %convolution_convert_fusion = bf16[2048,2048]{1,0:T(8,128)(2,1)} fusion(f32[2048,704]{0,1:T(8,128)} %fusion.7, bf16[2048,1408]{0,1:T(8,128)(2,1)} %all-gather.2.cloned.1.call-done, bf16[2048,2048]{1,0:T(8,128)(2,1)} %param.5, f32[2048]{0:T(1024)S(1)} %copy-done, f32[2048]{0:T(1024)S(1)} %add_rsqrt_fusion, bf16[16,704,128]{2,1,0:T(8,128)(2,1)S(1)} %all-to-all-done), kind=kOutput, calls=%fused_computation.5 | convolution fusion | flops 11840782336 | bytes 28327936 | tf_op jit(solution)/shard_map/dot_general | solution.py:40
  132.7 0.0 reduce-scatter.2.cloned.1.call-update
  132.7 52.6 %reduce-scatter.2.cloned.1.call-done = bf16[256,2048]{1,0:T(8,128)(2,1)} async-done(((bf16[2048,2048]{1,0:T(8,128)(2,1)}), bf16[256,2048]{1,0:T(8,128)(2,1)}) %reduce-scatter.2.cloned.1.call-update) | async-done | bytes 1048592 | tf_op jit(solution)/shard_map/reduce_scatter | solution.py:39
  (1 shorter events, 0.0 us)
Async XLA Ops:
  6.5 95.7 %all-gather.2.cloned.1.call-start = ((), (), s32[]{:S(2)}) async-start(), calls=%async_computation.2 | async-start | bytes 6127616 | tf_op jit(solution)/shard_map/all_gather | solution.py:10
  11.4 90.8 %copy-start = (f32[2048]{0:T(1024)S(1)}, f32[2048]{0:T(1024)}, u32[]{:S(2)}) copy-start(f32[2048]{0:T(1024)} %param.6) | copy-start | bytes 24580
  11.4 102.0 %all-to-all-start = ((bf16[16,704,128]{2,1,0:T(8,128)(2,1)}), bf16[16,704,128]{2,1,0:T(8,128)(2,1)S(1)}, u32[]{:S(2)}, u32[]{:S(2)}) async-start(bf16[16,704,128]{2,1,0:T(8,128)(2,1)} %broadcast_in_dim.2), calls=%async_computation | async-start | bytes 5767168 | tf_op jit(solution)/shard_map/all_to_all | solution.py:16
  20.1 165.3 %reduce-scatter.2.cloned.1.call-start = ((), (), s32[]{:S(2)}) async-start(), calls=%async_computation.3 | async-start | bytes 9437184 | tf_op jit(solution)/shard_map/reduce_scatter | solution.py:39
Sparse Core Ops, SparseCore 0:
  9.4 92.7 all-gather.1
  132.9 52.4 reduce-scatter.1
where the time goes:
time: 192 us
  waiting for transfers between devices  129 us (67%)
  matrix products  30.5 us (16%)
  between operations  13.4 us (7%)
  starting transfers between devices  8.76 us (5%)
  other arithmetic  7.1 us (4%)
  local copies, waits for them, and re-layouts  3.06 us (2%)
    all_gather x1, waiting for transfers between devices, side_by_side(): whole = lax.all_gather(both, axis, axis=dim, tiled=True)  76.7 us
    reduce_scatter x1, waiting for transfers between devices, per_device(): lax.psum_scatter(jnp.dot(hidden, down_full, preferred_element_type=jnp.fl...  52.6 us
    dot_general x1, matrix products, per_device(): jnp.dot(hidden, down_full, preferred_element_type=jnp.float32)  19.3 us
    dot_general x1, matrix products, per_device(): gate = jnp.dot(normed, gate_full, preferred_element_type=jnp.float32)  11.2 us
    all_to_all x1, starting transfers between devices, from_everyone(): return lax.all_to_all(copies, axis, split_axis=0, concat_axis=0, tiled=True)  8.72 us
    reduce_sum x1, other arithmetic, per_device(): scale = lax.rsqrt(jnp.mean(xf * xf, axis=-1, keepdims=True) + 1e-06)  5.32 us
  transfers between devices with their start and end apart: 3, of which 2 were waited for; matrix products, arithmetic and copies ran while one was open for 10% of the time, Pallas kernels for 0%

commit v1 on v0

v1 whole, which is shorter than its diff:
```python
import functools

import jax
import jax.numpy as jnp
from jax import lax
from jax.experimental import pallas as pl
from jax.experimental.pallas import tpu as pltpu
from jax.sharding import Mesh, PartitionSpec as P


D = 2048
LANES = 128
BLOCKS = 16
WIDTH = 704
ROWS = 256
CHUNKS = 4
PART = ROWS // CHUNKS
VMEM = pl.BlockSpec(memory_space=pltpu.VMEM)
SMEM = pl.BlockSpec(memory_space=pltpu.SMEM)
ANY = pl.BlockSpec(memory_space=pl.ANY)


def call(kernel, out, mib, **kw):
    return pl.pallas_call(kernel, out_shape=out, compiler_params=pltpu.CompilerParams(vmem_limit_bytes=mib << 20), **kw)


def masks(core):
    return (1, 3) if core == 0 else (3, 1)


def pair_up(value, axis, step):
    pairs = [(i * 2 + c, (i ^ masks(c)[step]) * 2 + c) for i in range(4) for c in range(2)]
    return lax.ppermute(value, (axis, "c"), pairs)


def double(block, route):
    have = block[None]
    for n, (axis, step) in enumerate(route):
        other = pair_up(have, axis, step)
        if n == 3:
            return have, other
        have = jnp.concatenate([have, other], axis=0)


def places(route, z, y, m):
    k = jnp.arange(BLOCKS, dtype=jnp.int32)
    at = {"z": jnp.full_like(k, z), "y": jnp.full_like(k, y)}
    for n, (axis, step) in enumerate(route):
        at[axis] = at[axis] ^ (((k >> n) & 1) * m[step])
    return at["z"] * 4 + at["y"]


ZZYY = (("z", 0), ("z", 1), ("y", 0), ("y", 1))
YYZZ = (("y", 0), ("y", 1), ("z", 0), ("z", 1))
ZYZY = (("z", 0), ("y", 0), ("z", 1), ("y", 1))
YZYZ = (("y", 0), ("z", 0), ("y", 1), ("z", 1))


def norm_kernel(rows, x_ref, gain_ref, out_ref):
    xf = x_ref[...].astype(jnp.float32)
    scale = lax.rsqrt(jnp.mean(xf * xf, axis=-1, keepdims=True) + 1e-06)
    out_ref[...] = (xf * scale * gain_ref[...]).astype(jnp.bfloat16)


def normalize(tokens, gain, rows):
    return call(
        norm_kernel, jax.ShapeDtypeStruct((2 * ROWS, D), jnp.bfloat16), 8,
        grid_spec=pltpu.PrefetchScalarGridSpec(
            num_scalar_prefetch=1,
            grid=(2,),
            in_specs=[pl.BlockSpec((ROWS, D), lambda i, rows: (rows[i], 0)), pl.BlockSpec((1, D), lambda i, rows: (0, 0))],
            out_specs=pl.BlockSpec((ROWS, D), lambda i, rows: (i, 0)),
        ),
    )(rows, tokens, gain.reshape(1, D))


def place_kernel(first, parts, *refs):
    cols, refs = refs[:parts], refs[parts:]
    ins, out_ref = refs[:parts], refs[-1]
    height = WIDTH // parts
    for n in range(parts):
        for k in range(8):
            at = pl.multiple_of(cols[n][first + k] * LANES, LANES)
            out_ref[n * height:(n + 1) * height, pl.ds(at, LANES)] = ins[n][k]


def place(cols, halves, first, into):
    parts = len(halves)
    shape = jax.ShapeDtypeStruct((WIDTH, D), jnp.bfloat16)
    more = [] if into is None else [into]
    return call(
        functools.partial(place_kernel, first, parts), shape, 8,
        in_specs=[SMEM] * parts + [VMEM] * (parts + len(more)), out_specs=VMEM,
        input_output_aliases={2 * parts: 0} if more else {},
    )(*cols, *halves, *more)


def nt(left, right):
    return lax.dot_general(left, right, (((1,), (1,)), ((), ())), preferred_element_type=jnp.float32)


def hidden_kernel(x_ref, gate_ref, up_ref, out_ref):
    x = x_ref[...]
    gate = nt(x, gate_ref[...])
    up = nt(x, up_ref[...])
    hidden = (gate / (1.0 + jnp.exp(-gate)) * up).astype(jnp.bfloat16)
    out_ref[...] = hidden.reshape(out_ref.shape)


def hidden_of(normed, gate, up):
    shape = jax.ShapeDtypeStruct((2, ROWS, WIDTH), jnp.bfloat16)
    return call(hidden_kernel, shape, 20, in_specs=[VMEM] * 3, out_specs=VMEM)(normed, gate, up)


def down_kernel(chunk, picks, n_hidden, at, *refs):
    hidden, down_ref, more, out_ref = refs[:n_hidden], refs[n_hidden], refs[n_hidden + 1:n_hidden + 1 + len(at)], refs[-1]
    rows = slice(chunk * PART, (chunk + 1) * PART)
    h = jnp.concatenate([hidden[i][j, rows, :] for i, j in picks], axis=0)
    for n in range(0, D, 512):
        part = jnp.dot(h, down_ref[:, n:n + 512], preferred_element_type=jnp.float32)
        for ref, start in zip(more, at):
            part = part + ref[start * PART:start * PART + h.shape[0], n:n + 512].astype(jnp.float32)
        out_ref[:, n:n + 512] = part.astype(jnp.bfloat16)


def down_of(chunk, hidden, picks, down, more, into=None):
    rows = len(picks) * PART
    kernel = functools.partial(down_kernel, chunk, picks, len(hidden), [m[1] for m in more])
    ins = [*hidden, down, *[m[0] for m in more]]
    specs = [VMEM] * len(ins)
    if into is None:
        return call(kernel, jax.ShapeDtypeStruct((rows, D), jnp.bfloat16), 12, in_specs=specs, out_specs=VMEM)(*ins)
    first = into is False
    return call(
        kernel, jax.ShapeDtypeStruct((ROWS, D), jnp.bfloat16), 12, grid=(1,),
        in_specs=specs + [] if first else specs + [ANY], out_specs=pl.BlockSpec((rows, D), lambda i: (chunk, 0)),
        input_output_aliases={} if first else {len(ins): 0},
    )(*ins, *([] if first else [into]))


def per_device(tokens, norm_gain, gate_weight, up_weight, down_weight):
    z, y, x, c = (lax.axis_index(a) for a in "zyxc")
    m1 = jnp.where(c == 0, 1, 3).astype(jnp.int32)
    m2 = 4 - m1
    m = (m1, m2)
    theirs = jnp.stack([x ^ m1 ^ m2, x ^ m2, x ^ m1, x]) * 2 + (1 - c)
    ours = jnp.stack([x ^ m1 ^ m2, x ^ m1, x ^ m2, x]) * 2 + c
    order = jnp.concatenate([theirs, ours]).astype(jnp.int32)

    gate = double(gate_weight.T, ZZYY)
    up = double(up_weight.T, YYZZ)
    half = WIDTH // 2
    down = [double(down_weight[:half], ZYZY), double(down_weight[half:], YZYZ)]

    gc, uc = places(ZZYY, z, y, m), places(YYZZ, z, y, m)
    dc = [places(ZYZY, z, y, m), places(YZYZ, z, y, m)]
    normed = [normalize(tokens, norm_gain, order[2 * i:2 * i + 2]) for i in range(4)]
    gw = place([gc], gate[:1], 0, None)
    gw = place([gc], gate[1:], 8, gw)
    uw = place([uc], up[:1], 0, None)
    uw = place([uc], up[1:], 8, uw)
    dw = place(dc, [d[0] for d in down], 0, None)
    dw = place(dc, [d[1] for d in down], 8, dw)
    hid = [hidden_of(normed[i], gw, uw) for i in range(4)]

    out = False
    for n in range(CHUNKS):
        sent = down_of(n, hid[:2], [(0, 0), (0, 1), (1, 0), (1, 1)], dw, [])
        got = lax.ppermute(sent, "c", [(0, 1), (1, 0)])
        sent = down_of(n, hid[2:3], [(0, 0), (0, 1)], dw, [(got, 0)])
        got1 = pair_up(sent, "x", 0)
        sent = down_of(n, hid[3:], [(0, 0)], dw, [(got, 2), (got1, 0)])
        got2 = pair_up(sent, "x", 1)
        out = down_of(n, hid[3:], [(0, 1)], dw, [(got, 3), (got1, 1), (got2, 0)], out)
    return out


def solution(mesh):
    torus = Mesh(mesh.devices.reshape(4, 4, 4, 2), ("z", "y", "x", "c"))
    fs, tp = ("z", "y"), ("x", "c")
    placed = (P(fs, None), P(), P(fs, tp), P(fs, tp), P(tp, fs))
    return jax.shard_map(per_device, mesh=torus, in_specs=placed, out_specs=P(fs + tp, None), check_vma=False)
```

time: 192 us -> 146 us (0.76)
  the two profiles are of different devices: /device:TPU:1 before, /device:TPU:0 now
where the time goes in v1:
time: 146 us
  waiting for transfers between devices  55.4 us (38%)
  Pallas kernels  42.7 us (29%)
  starting transfers between devices  39.2 us (27%)
  other arithmetic  4.45 us (3%)
  local copies, waits for them, and re-layouts  3.58 us (2%)
    ppermute x24, waiting for transfers between devices, pair_up(): return lax.ppermute(value, (axis, 'c'), pairs)  55.4 us
    ppermute x24, starting transfers between devices, pair_up(): return lax.ppermute(value, (axis, 'c'), pairs)  37.7 us
    pallas_call x4, Pallas kernels, hidden_of(): call(hidden_kernel, shape, 20, in_specs=[VMEM] * 3, out_specs=VMEM)  13.8 us
    pallas_call x6, Pallas kernels, place(): call(functools.partial(place_kernel, first, parts), shape, 8, in_specs=[S...  8.99 us
    pallas_call x12, Pallas kernels, down_of(): call(kernel, jax.ShapeDtypeStruct((rows, D), jnp.bfloat16), 12, in_specs=...  8.83 us
    pallas_call x4, Pallas kernels, normalize(): call(norm_kernel, jax.ShapeDtypeStruct((2 * ROWS, D), jnp.bfloat16), 8, g...  5.59 us
    pallas_call x4, Pallas kernels, down_of(): call(kernel, jax.ShapeDtypeStruct((ROWS, D), jnp.bfloat16), 12, grid=(1,)...  5.48 us
    concatenate x12, other arithmetic, double(): have = jnp.concatenate([have, other], axis=0)  4.34 us
  transfers between devices with their start and end apart: 28, of which 13 were waited for; matrix products, arithmetic and copies ran while one was open for 3% of the time, Pallas kernels for 22%

profile of v1, /device:TPU:0, one launch (start us, length us, event | category | flops | bytes accessed | tf_op | source)
XLA Modules:
  0.0 145.8 jit_solution(5594042028333793324)
XLA Ops:
  0.0 2.0 %collective-permute-start = (bf16[1,704,128]{2,1,0:T(8,128)(2,1)}, bf16[1,704,128]{2,1,0:T(8,128)(2,1)S(1)}, u32[]{:S(2)}, u32[]{:S(2)}) collective-permute-start(bf16[1,704,128]{2,1,0:T(8,128)(2,1)} %bitcast.21), channel_id=1, source_target_pairs={{0,32},{1,97},{32,0},{33,65},{64,96},{65,33},{96,64},{97,1},{2,34}... | collective-permute-start | bytes 540680 | tf_op jit(solution)/shard_map/ppermute | solution.py:33
  2.0 1.6 %collective-permute-start.4 = (bf16[1,704,128]{2,1,0:T(8,128)(2,1)}, bf16[1,704,128]{2,1,0:T(8,128)(2,1)S(1)}, u32[]{:S(2)}, u32[]{:S(2)}) collective-permute-start(bf16[1,704,128]{2,1,0:T(8,128)(2,1)} %bitcast.25), channel_id=1, source_target_pairs={{0,8},{1,25},{8,0},{9,17},{16,24},{17,9},{24,16},{25,1},{2,10},{3,... | collective-permute-start | bytes 540680 | tf_op jit(solution)/shard_map/ppermute | solution.py:33
  3.6 2.2 %collective-permute-done = bf16[1,704,128]{2,1,0:T(8,128)(2,1)S(1)} collective-permute-done((bf16[1,704,128]{2,1,0:T(8,128)(2,1)}, bf16[1,704,128]{2,1,0:T(8,128)(2,1)S(1)}, u32[]{:S(2)}, u32[]{:S(2)}) %collective-permute-start) | collective-permute-done | bytes 180256 | tf_op jit(solution)/shard_map/ppermute | solution.py:33
  5.8 1.0 pad_maximum_fusion.6
  6.7 4.2 %collective-permute-start.1 = (bf16[2,704,128]{2,1,0:T(8,128)(2,1)S(1)}, bf16[2,704,128]{2,1,0:T(8,128)(2,1)S(1)}, u32[]{:S(2)}, u32[]{:S(2)}) collective-permute-start(bf16[2,704,128]{2,1,0:T(8,128)(2,1)S(1)} %pad_maximum_fusion.6), channel_id=1, source_target_pairs={{0,96},{1,33},{32,64},{33,1},{64,32},{65,97},{96,0},{97,65},{2,98}... | collective-permute-start | bytes 1081352 | tf_op jit(solution)/shard_map/ppermute | solution.py:33
  10.9 1.0 pad_maximum_fusion.7
  11.9 3.1 %collective-permute-start.5 = (bf16[2,704,128]{2,1,0:T(8,128)(2,1)S(1)}, bf16[2,704,128]{2,1,0:T(8,128)(2,1)S(1)}, u32[]{:S(2)}, u32[]{:S(2)}) collective-permute-start(bf16[2,704,128]{2,1,0:T(8,128)(2,1)S(1)} %pad_maximum_fusion.7), channel_id=1, source_target_pairs={{0,24},{1,9},{8,16},{9,1},{16,8},{17,25},{24,0},{25,17},{2,26},{3,... | collective-permute-start | bytes 1081352 | tf_op jit(solution)/shard_map/ppermute | solution.py:33
  15.0 1.3 collective-permute-done.1
  16.4 1.7 %collective-permute-start.2 = (bf16[4,704,128]{2,1,0:T(8,128)(2,1)S(1)}, bf16[4,704,128]{2,1,0:T(8,128)(2,1)S(1)}, u32[]{:S(2)}, u32[]{:S(2)}) collective-permute-start(bf16[4,704,128]{2,1,0:T(8,128)(2,1)S(1)} %pad_maximum_fusion.2), channel_id=1, source_target_pairs={{0,8},{1,25},{8,0},{9,17},{16,24},{17,9},{24,16},{25,1},{2,10},{3,... | collective-permute-start | bytes 2162696 | tf_op jit(solution)/shard_map/ppermute | solution.py:33
  18.0 4.6 %collective-permute-done.5 = bf16[2,704,128]{2,1,0:T(8,128)(2,1)S(1)} collective-permute-done((bf16[2,704,128]{2,1,0:T(8,128)(2,1)S(1)}, bf16[2,704,128]{2,1,0:T(8,128)(2,1)S(1)}, u32[]{:S(2)}, u32[]{:S(2)}) %collective-permute-start.5) | collective-permute-done | bytes 360480 | tf_op jit(solution)/shard_map/ppermute | solution.py:33
  22.9 2.1 %collective-permute-start.8 = (bf16[1,352,128]{2,1,0:T(8,128)(2,1)S(1)}, bf16[1,352,128]{2,1,0:T(8,128)(2,1)S(1)}, u32[]{:S(2)}, u32[]{:S(2)}) collective-permute-start(bf16[1,352,128]{2,1,0:T(8,128)(2,1)S(1)} %get-tuple-element.6), channel_id=1, source_target_pairs={{0,32},{1,97},{32,0},{33,65},{64,96},{65,33},{96,64},{97,1},{2,34}... | collective-permute-start | bytes 270344 | tf_op jit(solution)/shard_map/ppermute | solution.py:33
  25.4 9.7 %collective-permute-done.8 = bf16[1,352,128]{2,1,0:T(8,128)(2,1)S(1)} collective-permute-done((bf16[1,352,128]{2,1,0:T(8,128)(2,1)S(1)}, bf16[1,352,128]{2,1,0:T(8,128)(2,1)S(1)}, u32[]{:S(2)}, u32[]{:S(2)}) %collective-permute-start.8) | collective-permute-done | bytes 90144 | tf_op jit(solution)/shard_map/ppermute | solution.py:33
  35.9 2.8 %collective-permute-start.3 = (bf16[8,704,128]{2,1,0:T(8,128)(2,1)S(1)}, bf16[8,704,128]{2,1,0:T(8,128)(2,1)}, u32[]{:S(2)}, u32[]{:S(2)}) collective-permute-start(bf16[8,704,128]{2,1,0:T(8,128)(2,1)S(1)} %pad_maximum_fusion.refs_1_), channel_id=1, source_target_pairs={{0,24},{1,9},{8,16},{9,1},{16,8},{17,25},{24,0},{25,17},{2,26},{3,... | collective-permute-start | bytes 4325384 | tf_op jit(solution)/shard_map/ppermute | solution.py:33
  38.9 3.7 %collective-permute-done.9 = bf16[2,352,128]{2,1,0:T(8,128)(2,1)S(1)} collective-permute-done((bf16[2,352,128]{2,1,0:T(8,128)(2,1)S(1)}, bf16[2,352,128]{2,1,0:T(8,128)(2,1)S(1)}, u32[]{:S(2)}, u32[]{:S(2)}) %collective-permute-start.9) | collective-permute-done | bytes 180256 | tf_op jit(solution)/shard_map/ppermute | solution.py:33
  43.2 2.8 %collective-permute-start.14 = (bf16[4,352,128]{2,1,0:T(8,128)(2,1)S(1)}, bf16[4,352,128]{2,1,0:T(8,128)(2,1)S(1)}, u32[]{:S(2)}, u32[]{:S(2)}) collective-permute-start(bf16[4,352,128]{2,1,0:T(8,128)(2,1)S(1)} %pad_maximum_fusion.9), channel_id=1, source_target_pairs={{0,24},{1,9},{8,16},{9,1},{16,8},{17,25},{24,0},{25,17},{2,26},{3,... | collective-permute-start | bytes 1081352 | tf_op jit(solution)/shard_map/ppermute | solution.py:33
  46.0 17.0 %collective-permute-done.10 = bf16[4,352,128]{2,1,0:T(8,128)(2,1)S(1)} collective-permute-done((bf16[4,352,128]{2,1,0:T(8,128)(2,1)S(1)}, bf16[4,352,128]{2,1,0:T(8,128)(2,1)S(1)}, u32[]{:S(2)}, u32[]{:S(2)}) %collective-permute-start.10) | collective-permute-done | bytes 360480 | tf_op jit(solution)/shard_map/ppermute | solution.py:33
  63.0 0.9 pad_maximum_fusion.4.refs_2_
  64.5 1.0 pad_maximum_fusion.5.refs_3_
  65.6 3.4 %copy-done = bf16[2048,2048]{1,0:T(8,128)(2,1)S(1)} copy-done((bf16[2048,2048]{1,0:T(8,128)(2,1)S(1)}, bf16[2048,2048]{1,0:T(8,128)(2,1)}, u32[]{:S(2)}) %copy-start) | copy-done | bytes 8388632
  69.0 1.4 shard_map.63.x_ref
  70.4 1.4 shard_map.65.x_ref
  71.8 1.7 %shard_map.61.refs_4_ = bf16[704,2048]{1,0:T(8,128)(2,1)S(1)} custom-call(s32[16]{0:T(128)S(1)} %get-tuple-element.12.refs_0_, s32[16]{0:T(128)S(1)} %get-tuple-element.11.refs_1_, bf16[8,352,128]{2,1,0:T(8,128)(2,1)} %pad_maximum_fusion.4.refs_2_, bf16[8,352,128]{2,1,0:T(8,128)(2,1)} %pad_maximum_fusion.5.refs_3_), custom_call_target="tpu_custom_call" | custom-call | tf_op jit(solution)/shard_map/pallas_call | solution.py:91
  73.6 1.0 shard_map.56.refs_2_
  74.5 1.0 shard_map.58.refs_2_
  75.5 1.2 collective-permute-done.11.refs_2_
  76.7 1.5 %collective-permute-done.15.refs_3_ = bf16[8,352,128]{2,1,0:T(8,128)(2,1)} collective-permute-done((bf16[8,352,128]{2,1,0:T(8,128)(2,1)}, bf16[8,352,128]{2,1,0:T(8,128)(2,1)}, u32[]{:S(2)}, u32[]{:S(2)}) %collective-permute-start.15) | collective-permute-done | bytes 720928 | tf_op jit(solution)/shard_map/ppermute | solution.py:33
  78.2 1.7 %shard_map.62.refs_2_.refs_1_ = bf16[704,2048]{1,0:T(8,128)(2,1)S(1)} custom-call(s32[16]{0:T(128)S(1)} %get-tuple-element.12.refs_0_, s32[16]{0:T(128)S(1)} %get-tuple-element.11.refs_1_, bf16[8,352,128]{2,1,0:T(8,128)(2,1)} %collective-permute-done.11.refs_2_, ...), custom_call_target="tpu_custom_call", output_to_operand_aliasing={{}: (4, {})} | custom-call | tf_op jit(solution)/shard_map/pallas_call | solution.py:91
  80.0 1.8 %shard_map.57.gate_ref = bf16[704,2048]{1,0:T(8,128)(2,1)S(1)} custom-call(s32[16]{0:T(128)S(1)} %get-tuple-element.14.refs_0_, bf16[8,704,128]{2,1,0:T(8,128)(2,1)} %collective-permute-done.3.refs_1_, bf16[704,2048]{1,0:T(8,128)(2,1)S(1)} %shard_map.56.refs_2_), custom_call_target="tpu_custom_call", output_to_operand_aliasing={{}: (2, {})} | custom-call | tf_op jit(solution)/shard_map/pallas_call | solution.py:91
  81.8 1.8 %shard_map.59.up_ref = bf16[704,2048]{1,0:T(8,128)(2,1)S(1)} custom-call(s32[16]{0:T(128)S(1)} %get-tuple-element.13.refs_0_, bf16[8,704,128]{2,1,0:T(8,128)(2,1)} %collective-permute-done.7.refs_1_, bf16[704,2048]{1,0:T(8,128)(2,1)S(1)} %shard_map.58.refs_2_), custom_call_target="tpu_custom_call", output_to_operand_aliasing={{}: (2, {})} | custom-call | tf_op jit(solution)/shard_map/pallas_call | solution.py:91
  83.6 3.5 %shard_map.64.refs_0_ = bf16[2,256,704]{2,1,0:T(8,128)(2,1)S(1)} custom-call(bf16[512,2048]{1,0:T(8,128)(2,1)S(1)} %shard_map.63.x_ref, bf16[704,2048]{1,0:T(8,128)(2,1)S(1)} %shard_map.57.gate_ref, bf16[704,2048]{1,0:T(8,128)(2,1)S(1)} %shard_map.59.up_ref), custom_call_target="tpu_custom_call" | custom-call | tf_op jit(solution)/shard_map/pallas_call | solution.py:112
  87.0 3.5 %shard_map.66.refs_1_ = bf16[2,256,704]{2,1,0:T(8,128)(2,1)S(1)} custom-call(bf16[512,2048]{1,0:T(8,128)(2,1)S(1)} %shard_map.65.x_ref, bf16[704,2048]{1,0:T(8,128)(2,1)S(1)} %shard_map.57.gate_ref, bf16[704,2048]{1,0:T(8,128)(2,1)S(1)} %shard_map.59.up_ref), custom_call_target="tpu_custom_call" | custom-call | tf_op jit(solution)/shard_map/pallas_call | solution.py:112
  90.5 1.0 shard_map.75
  91.6 1.0 shard_map.78
  92.6 0.6 collective-permute-start.25
  93.2 1.0 shard_map.72
  94.3 1.0 shard_map.67
  95.2 0.8 collective-permute-start.16
  96.1 1.4 shard_map.68.x_ref
  97.5 3.5 %shard_map.69.refs_0_ = bf16[2,256,704]{2,1,0:T(8,128)(2,1)S(1)} custom-call(bf16[512,2048]{1,0:T(8,128)(2,1)S(1)} %shard_map.68.x_ref, bf16[704,2048]{1,0:T(8,128)(2,1)S(1)} %shard_map.57.gate_ref, bf16[704,2048]{1,0:T(8,128)(2,1)S(1)} %shard_map.59.up_ref), custom_call_target="tpu_custom_call" | custom-call | tf_op jit(solution)/shard_map/pallas_call | solution.py:112
  101.0 0.6 shard_map.76
  101.6 1.6 %collective-permute-start.23 = (bf16[128,2048]{1,0:T(8,128)(2,1)S(1)}, bf16[128,2048]{1,0:T(8,128)(2,1)S(1)}, u32[]{:S(2)}, u32[]{:S(2)}) collective-permute-start(bf16[128,2048]{1,0:T(8,128)(2,1)S(1)} %shard_map.76), channel_id=1, source_target_pairs={{0,2},{1,7},{2,0},{3,5},{4,6},{5,3},{6,4},{7,1},{8,10},{9,15},{10,... | collective-permute-start | bytes 1572872 | tf_op jit(solution)/shard_map/ppermute | solution.py:33
  103.2 0.6 shard_map.79
  103.7 0.6 collective-permute-start.26
  104.4 0.6 shard_map.73
  105.0 1.6 %collective-permute-start.20 = (bf16[128,2048]{1,0:T(8,128)(2,1)S(1)}, bf16[128,2048]{1,0:T(8,128)(2,1)S(1)}, u32[]{:S(2)}, u32[]{:S(2)}) collective-permute-start(bf16[128,2048]{1,0:T(8,128)(2,1)S(1)} %shard_map.73), channel_id=1, source_target_pairs={{0,2},{1,7},{2,0},{3,5},{4,6},{5,3},{6,4},{7,1},{8,10},{9,15},{10,... | collective-permute-start | bytes 1572872 | tf_op jit(solution)/shard_map/ppermute | solution.py:33
  106.5 0.6 shard_map.70
  107.1 0.6 collective-permute-start.17
  107.7 1.4 shard_map.55.x_ref
  109.1 3.5 %shard_map.60.refs_0_ = bf16[2,256,704]{2,1,0:T(8,128)(2,1)S(1)} custom-call(bf16[512,2048]{1,0:T(8,128)(2,1)S(1)} %shard_map.55.x_ref, bf16[704,2048]{1,0:T(8,128)(2,1)S(1)} %shard_map.57.gate_ref, bf16[704,2048]{1,0:T(8,128)(2,1)S(1)} %shard_map.59.up_ref), custom_call_target="tpu_custom_call" | custom-call | tf_op jit(solution)/shard_map/pallas_call | solution.py:112
  112.6 0.6 shard_map.77
  113.3 2.8 %collective-permute-start.24 = (bf16[64,2048]{1,0:T(8,128)(2,1)S(1)}, bf16[64,2048]{1,0:T(8,128)(2,1)S(1)}, u32[]{:S(2)}, u32[]{:S(2)}) collective-permute-start(bf16[64,2048]{1,0:T(8,128)(2,1)S(1)} %shard_map.77), channel_id=1, source_target_pairs={{0,6},{1,3},{2,4},{3,1},{4,2},{5,7},{6,0},{7,5},{8,14},{9,11},{10,... | collective-permute-start | bytes 786440 | tf_op jit(solution)/shard_map/ppermute | solution.py:33
  116.4 0.6 shard_map.80
  117.1 2.8 %collective-permute-start.27 = (bf16[64,2048]{1,0:T(8,128)(2,1)S(1)}, bf16[64,2048]{1,0:T(8,128)(2,1)S(1)}, u32[]{:S(2)}, u32[]{:S(2)}) collective-permute-start(bf16[64,2048]{1,0:T(8,128)(2,1)S(1)} %shard_map.80), channel_id=1, source_target_pairs={{0,6},{1,3},{2,4},{3,1},{4,2},{5,7},{6,0},{7,5},{8,14},{9,11},{10,... | collective-permute-start | bytes 786440 | tf_op jit(solution)/shard_map/ppermute | solution.py:33
  119.9 6.9 %collective-permute-done.20.refs_3_ = bf16[128,2048]{1,0:T(8,128)(2,1)S(1)} collective-permute-done((bf16[128,2048]{1,0:T(8,128)(2,1)S(1)}, bf16[128,2048]{1,0:T(8,128)(2,1)S(1)}, u32[]{:S(2)}, u32[]{:S(2)}) %collective-permute-start.20) | collective-permute-done | bytes 524320 | tf_op jit(solution)/shard_map/ppermute | solution.py:33
  126.9 0.6 shard_map.74
  127.5 2.8 %collective-permute-start.21 = (bf16[64,2048]{1,0:T(8,128)(2,1)S(1)}, bf16[64,2048]{1,0:T(8,128)(2,1)S(1)}, u32[]{:S(2)}, u32[]{:S(2)}) collective-permute-start(bf16[64,2048]{1,0:T(8,128)(2,1)S(1)} %shard_map.74), channel_id=1, source_target_pairs={{0,6},{1,3},{2,4},{3,1},{4,2},{5,7},{6,0},{7,5},{8,14},{9,11},{10,... | collective-permute-start | bytes 786440 | tf_op jit(solution)/shard_map/ppermute | solution.py:33
  130.4 5.8 %collective-permute-done.17.refs_3_ = bf16[128,2048]{1,0:T(8,128)(2,1)S(1)} collective-permute-done((bf16[128,2048]{1,0:T(8,128)(2,1)S(1)}, bf16[128,2048]{1,0:T(8,128)(2,1)S(1)}, u32[]{:S(2)}, u32[]{:S(2)}) %collective-permute-start.17) | collective-permute-done | bytes 524320 | tf_op jit(solution)/shard_map/ppermute | solution.py:33
  136.1 0.6 shard_map.71
  136.8 2.8 %collective-permute-start.18 = (bf16[64,2048]{1,0:T(8,128)(2,1)S(1)}, bf16[64,2048]{1,0:T(8,128)(2,1)S(1)}, u32[]{:S(2)}, u32[]{:S(2)}) collective-permute-start(bf16[64,2048]{1,0:T(8,128)(2,1)S(1)} %shard_map.71), channel_id=1, source_target_pairs={{0,6},{1,3},{2,4},{3,1},{4,2},{5,7},{6,0},{7,5},{8,14},{9,11},{10,... | collective-permute-start | bytes 786440 | tf_op jit(solution)/shard_map/ppermute | solution.py:33
  139.6 1.4 shard_map.81.refs_5_
  141.0 1.4 shard_map.82.refs_5_
  142.3 1.4 shard_map.83.refs_5_
  143.7 0.7 collective-permute-done.18.refs_4_
  144.4 1.4 shard_map.84
  (55 shorter events, 3.7 us)
Async XLA Ops:
  0.0 16.3 %copy-start.2 = (bf16[128,704]{0,1:T(8,128)(2,1)S(1)}, bf16[128,704]{0,1:T(8,128)(2,1)}, u32[]{:S(2)}) copy-start(bf16[128,704]{0,1:T(8,128)(2,1)} %param.7) | copy-start | bytes 540676
  0.0 5.8 %collective-permute-start = (bf16[1,704,128]{2,1,0:T(8,128)(2,1)}, bf16[1,704,128]{2,1,0:T(8,128)(2,1)S(1)}, u32[]{:S(2)}, u32[]{:S(2)}) collective-permute-start(bf16[1,704,128]{2,1,0:T(8,128)(2,1)} %bitcast.21), channel_id=1, source_target_pairs={{0,32},{1,97},{32,0},{33,65},{64,96},{65,33},{96,64},{97,1},{2,34}... | collective-permute-start | bytes 540680 | tf_op jit(solution)/shard_map/ppermute | solution.py:33
  2.0 20.6 %copy-start.3 = (bf16[128,704]{0,1:T(8,128)(2,1)S(1)}, bf16[128,704]{0,1:T(8,128)(2,1)}, u32[]{:S(2)}) copy-start(bf16[128,704]{0,1:T(8,128)(2,1)} %param.8) | copy-start | bytes 540676
  2.0 8.9 %collective-permute-start.4 = (bf16[1,704,128]{2,1,0:T(8,128)(2,1)}, bf16[1,704,128]{2,1,0:T(8,128)(2,1)S(1)}, u32[]{:S(2)}, u32[]{:S(2)}) collective-permute-start(bf16[1,704,128]{2,1,0:T(8,128)(2,1)} %bitcast.25), channel_id=1, source_target_pairs={{0,8},{1,25},{8,0},{9,17},{16,24},{17,9},{24,16},{25,1},{2,10},{3,... | collective-permute-start | bytes 540680 | tf_op jit(solution)/shard_map/ppermute | solution.py:33
  6.7 9.6 %collective-permute-start.1 = (bf16[2,704,128]{2,1,0:T(8,128)(2,1)S(1)}, bf16[2,704,128]{2,1,0:T(8,128)(2,1)S(1)}, u32[]{:S(2)}, u32[]{:S(2)}) collective-permute-start(bf16[2,704,128]{2,1,0:T(8,128)(2,1)S(1)} %pad_maximum_fusion.6), channel_id=1, source_target_pairs={{0,96},{1,33},{32,64},{33,1},{64,32},{65,97},{96,0},{97,65},{2,98}... | collective-permute-start | bytes 1081352 | tf_op jit(solution)/shard_map/ppermute | solution.py:33
  11.9 11.0 %copy-start.4 = (bf16[704,128]{1,0:T(8,128)(2,1)S(1)}, bf16[704,128]{1,0:T(8,128)(2,1)}, u32[]{:S(2)}) copy-start(bf16[704,128]{1,0:T(8,128)(2,1)} %param.9) | copy-start | bytes 540676
  11.9 10.8 %collective-permute-start.5 = (bf16[2,704,128]{2,1,0:T(8,128)(2,1)S(1)}, bf16[2,704,128]{2,1,0:T(8,128)(2,1)S(1)}, u32[]{:S(2)}, u32[]{:S(2)}) collective-permute-start(bf16[2,704,128]{2,1,0:T(8,128)(2,1)S(1)} %pad_maximum_fusion.7), channel_id=1, source_target_pairs={{0,24},{1,9},{8,16},{9,1},{16,8},{17,25},{24,0},{25,17},{2,26},{3,... | collective-permute-start | bytes 1081352 | tf_op jit(solution)/shard_map/ppermute | solution.py:33
  16.4 19.3 %collective-permute-start.2 = (bf16[4,704,128]{2,1,0:T(8,128)(2,1)S(1)}, bf16[4,704,128]{2,1,0:T(8,128)(2,1)S(1)}, u32[]{:S(2)}, u32[]{:S(2)}) collective-permute-start(bf16[4,704,128]{2,1,0:T(8,128)(2,1)S(1)} %pad_maximum_fusion.2), channel_id=1, source_target_pairs={{0,8},{1,25},{8,0},{9,17},{16,24},{17,9},{24,16},{25,1},{2,10},{3,... | collective-permute-start | bytes 2162696 | tf_op jit(solution)/shard_map/ppermute | solution.py:33
  22.7 15.9 %collective-permute-start.6 = (bf16[4,704,128]{2,1,0:T(8,128)(2,1)S(1)}, bf16[4,704,128]{2,1,0:T(8,128)(2,1)S(1)}, u32[]{:S(2)}, u32[]{:S(2)}) collective-permute-start(bf16[4,704,128]{2,1,0:T(8,128)(2,1)S(1)} %pad_maximum_fusion.3), channel_id=1, source_target_pairs={{0,32},{1,97},{32,0},{33,65},{64,96},{65,33},{96,64},{97,1},{2,34}... | collective-permute-start | bytes 2162696 | tf_op jit(solution)/shard_map/ppermute | solution.py:33
  22.9 12.2 %collective-permute-start.8 = (bf16[1,352,128]{2,1,0:T(8,128)(2,1)S(1)}, bf16[1,352,128]{2,1,0:T(8,128)(2,1)S(1)}, u32[]{:S(2)}, u32[]{:S(2)}) collective-permute-start(bf16[1,352,128]{2,1,0:T(8,128)(2,1)S(1)} %get-tuple-element.6), channel_id=1, source_target_pairs={{0,32},{1,97},{32,0},{33,65},{64,96},{65,33},{96,64},{97,1},{2,34}... | collective-permute-start | bytes 270344 | tf_op jit(solution)/shard_map/ppermute | solution.py:33
  25.0 10.7 %collective-permute-start.12 = (bf16[1,352,128]{2,1,0:T(8,128)(2,1)S(1)}, bf16[1,352,128]{2,1,0:T(8,128)(2,1)S(1)}, u32[]{:S(2)}, u32[]{:S(2)}) collective-permute-start(bf16[1,352,128]{2,1,0:T(8,128)(2,1)S(1)} %get-tuple-element.5), channel_id=1, source_target_pairs={{0,8},{1,25},{8,0},{9,17},{16,24},{17,9},{24,16},{25,1},{2,10},{3,... | collective-permute-start | bytes 270344 | tf_op jit(solution)/shard_map/ppermute | solution.py:33
  35.1 7.5 %collective-permute-start.9 = (bf16[2,352,128]{2,1,0:T(8,128)(2,1)S(1)}, bf16[2,352,128]{2,1,0:T(8,128)(2,1)S(1)}, u32[]{:S(2)}, u32[]{:S(2)}) collective-permute-start(bf16[2,352,128]{2,1,0:T(8,128)(2,1)S(1)} %pad_maximum_fusion.10), channel_id=1, source_target_pairs={{0,8},{1,25},{8,0},{9,17},{16,24},{17,9},{24,16},{25,1},{2,10},{3,... | collective-permute-start | bytes 540680 | tf_op jit(solution)/shard_map/ppermute | solution.py:33
  35.6 7.5 %collective-permute-start.13 = (bf16[2,352,128]{2,1,0:T(8,128)(2,1)S(1)}, bf16[2,352,128]{2,1,0:T(8,128)(2,1)S(1)}, u32[]{:S(2)}, u32[]{:S(2)}) collective-permute-start(bf16[2,352,128]{2,1,0:T(8,128)(2,1)S(1)} %pad_maximum_fusion.11), channel_id=1, source_target_pairs={{0,32},{1,97},{32,0},{33,65},{64,96},{65,33},{96,64},{97,1},{2,34}... | collective-permute-start | bytes 540680 | tf_op jit(solution)/shard_map/ppermute | solution.py:33
  35.9 44.1 %collective-permute-start.3 = (bf16[8,704,128]{2,1,0:T(8,128)(2,1)S(1)}, bf16[8,704,128]{2,1,0:T(8,128)(2,1)}, u32[]{:S(2)}, u32[]{:S(2)}) collective-permute-start(bf16[8,704,128]{2,1,0:T(8,128)(2,1)S(1)} %pad_maximum_fusion.refs_1_), channel_id=1, source_target_pairs={{0,24},{1,9},{8,16},{9,1},{16,8},{17,25},{24,0},{25,17},{2,26},{3,... | collective-permute-start | bytes 4325384 | tf_op jit(solution)/shard_map/ppermute | solution.py:33
  38.8 43.0 %collective-permute-start.7 = (bf16[8,704,128]{2,1,0:T(8,128)(2,1)S(1)}, bf16[8,704,128]{2,1,0:T(8,128)(2,1)}, u32[]{:S(2)}, u32[]{:S(2)}) collective-permute-start(bf16[8,704,128]{2,1,0:T(8,128)(2,1)S(1)} %pad_maximum_fusion.1.refs_1_), channel_id=1, source_target_pairs={{0,96},{1,33},{32,64},{33,1},{64,32},{65,97},{96,0},{97,65},{2,98}... | collective-permute-start | bytes 4325384 | tf_op jit(solution)/shard_map/ppermute | solution.py:33
  42.6 20.3 %collective-permute-start.10 = (bf16[4,352,128]{2,1,0:T(8,128)(2,1)S(1)}, bf16[4,352,128]{2,1,0:T(8,128)(2,1)S(1)}, u32[]{:S(2)}, u32[]{:S(2)}) collective-permute-start(bf16[4,352,128]{2,1,0:T(8,128)(2,1)S(1)} %pad_maximum_fusion.8), channel_id=1, source_target_pairs={{0,96},{1,33},{32,64},{33,1},{64,32},{65,97},{96,0},{97,65},{2,98}... | collective-permute-start | bytes 1081352 | tf_op jit(solution)/shard_map/ppermute | solution.py:33
  43.2 22.4 %copy-start.1 = (f32[2048]{0:T(1024)S(1)}, f32[2048]{0:T(1024)}, u32[]{:S(2)}) copy-start(f32[2048]{0:T(1024)} %param.6) | copy-start | bytes 24580
  43.2 21.3 %collective-permute-start.14 = (bf16[4,352,128]{2,1,0:T(8,128)(2,1)S(1)}, bf16[4,352,128]{2,1,0:T(8,128)(2,1)S(1)}, u32[]{:S(2)}, u32[]{:S(2)}) collective-permute-start(bf16[4,352,128]{2,1,0:T(8,128)(2,1)S(1)} %pad_maximum_fusion.9), channel_id=1, source_target_pairs={{0,24},{1,9},{8,16},{9,1},{16,8},{17,25},{24,0},{25,17},{2,26},{3,... | collective-permute-start | bytes 1081352 | tf_op jit(solution)/shard_map/ppermute | solution.py:33
  63.9 12.8 %collective-permute-start.11 = (bf16[8,352,128]{2,1,0:T(8,128)(2,1)}, bf16[8,352,128]{2,1,0:T(8,128)(2,1)}, u32[]{:S(2)}, u32[]{:S(2)}) collective-permute-start(bf16[8,352,128]{2,1,0:T(8,128)(2,1)} %pad_maximum_fusion.4.refs_2_), channel_id=1, source_target_pairs={{0,24},{1,9},{8,16},{9,1},{16,8},{17,25},{24,0},{25,17},{2,26},{3,... | collective-permute-start | bytes 2162696 | tf_op jit(solution)/shard_map/ppermute | solution.py:33
  65.4 12.8 %collective-permute-start.15 = (bf16[8,352,128]{2,1,0:T(8,128)(2,1)}, bf16[8,352,128]{2,1,0:T(8,128)(2,1)}, u32[]{:S(2)}, u32[]{:S(2)}) collective-permute-start(bf16[8,352,128]{2,1,0:T(8,128)(2,1)} %pad_maximum_fusion.5.refs_3_), channel_id=1, source_target_pairs={{0,96},{1,33},{32,64},{33,1},{64,32},{65,97},{96,0},{97,65},{2,98}... | collective-permute-start | bytes 2162696 | tf_op jit(solution)/shard_map/ppermute | solution.py:33
  65.6 3.4 %copy-start = (bf16[2048,2048]{1,0:T(8,128)(2,1)S(1)}, bf16[2048,2048]{1,0:T(8,128)(2,1)}, u32[]{:S(2)}) copy-start(bf16[2048,2048]{1,0:T(8,128)(2,1)} %x_ref.7) | copy-start | bytes 25165828
  91.5 9.5 %collective-permute-start.22 = (bf16[256,2048]{1,0:T(8,128)(2,1)S(1)}, bf16[256,2048]{1,0:T(8,128)(2,1)S(1)}, u32[]{:S(2)}, u32[]{:S(2)}) collective-permute-start(bf16[256,2048]{1,0:T(8,128)(2,1)S(1)} %shard_map.75), channel_id=1, source_target_pairs={{0,1},{1,0},{2,3},{3,2},{4,5},{5,4},{6,7},{7,6},{8,9},{9,8},{10,11... | collective-permute-start | bytes 3145736 | tf_op jit(solution)/shard_map/ppermute | solution.py:169
  91.6 4.5 %slice-start = ((s8[8388608]{0:T(1024)(128)(4,1)}), s8[4194304]{0:T(1024)(128)(4,1)S(1)}, s32[]{:S(2)}) async-start(s8[8388608]{0:T(1024)(128)(4,1)} %bitcast.15), calls=%async_computation | async-start | bytes 8388608
  92.6 3.5 %slice-start.1 = ((s8[8388608]{0:T(1024)(128)(4,1)}), s8[4194304]{0:T(1024)(128)(4,1)S(1)}, s32[]{:S(2)}) async-start(s8[8388608]{0:T(1024)(128)(4,1)} %bitcast.15), calls=%async_computation.1 | async-start | bytes 8388608
  92.6 10.6 %collective-permute-start.25 = (bf16[256,2048]{1,0:T(8,128)(2,1)S(1)}, bf16[256,2048]{1,0:T(8,128)(2,1)S(1)}, u32[]{:S(2)}, u32[]{:S(2)}) collective-permute-start(bf16[256,2048]{1,0:T(8,128)(2,1)S(1)} %shard_map.78), channel_id=1, source_target_pairs={{0,1},{1,0},{2,3},{3,2},{4,5},{5,4},{6,7},{7,6},{8,9},{9,8},{10,11... | collective-permute-start | bytes 3145736 | tf_op jit(solution)/shard_map/ppermute | solution.py:169
  94.1 10.2 %collective-permute-start.19 = (bf16[256,2048]{1,0:T(8,128)(2,1)S(1)}, bf16[256,2048]{1,0:T(8,128)(2,1)S(1)}, u32[]{:S(2)}, u32[]{:S(2)}) collective-permute-start(bf16[256,2048]{1,0:T(8,128)(2,1)S(1)} %shard_map.72), channel_id=1, source_target_pairs={{0,1},{1,0},{2,3},{3,2},{4,5},{5,4},{6,7},{7,6},{8,9},{9,8},{10,11... | collective-permute-start | bytes 3145736 | tf_op jit(solution)/shard_map/ppermute | solution.py:169
  95.2 11.3 %collective-permute-start.16 = (bf16[256,2048]{1,0:T(8,128)(2,1)S(1)}, bf16[256,2048]{1,0:T(8,128)(2,1)S(1)}, u32[]{:S(2)}, u32[]{:S(2)}) collective-permute-start(bf16[256,2048]{1,0:T(8,128)(2,1)S(1)} %shard_map.67), channel_id=1, source_target_pairs={{0,1},{1,0},{2,3},{3,2},{4,5},{5,4},{6,7},{7,6},{8,9},{9,8},{10,11... | collective-permute-start | bytes 3145736 | tf_op jit(solution)/shard_map/ppermute | solution.py:169
  101.6 11.0 %collective-permute-start.23 = (bf16[128,2048]{1,0:T(8,128)(2,1)S(1)}, bf16[128,2048]{1,0:T(8,128)(2,1)S(1)}, u32[]{:S(2)}, u32[]{:S(2)}) collective-permute-start(bf16[128,2048]{1,0:T(8,128)(2,1)S(1)} %shard_map.76), channel_id=1, source_target_pairs={{0,2},{1,7},{2,0},{3,5},{4,6},{5,3},{6,4},{7,1},{8,10},{9,15},{10,... | collective-permute-start | bytes 1572872 | tf_op jit(solution)/shard_map/ppermute | solution.py:33
  103.7 12.7 %collective-permute-start.26 = (bf16[128,2048]{1,0:T(8,128)(2,1)S(1)}, bf16[128,2048]{1,0:T(8,128)(2,1)S(1)}, u32[]{:S(2)}, u32[]{:S(2)}) collective-permute-start(bf16[128,2048]{1,0:T(8,128)(2,1)S(1)} %shard_map.79), channel_id=1, source_target_pairs={{0,2},{1,7},{2,0},{3,5},{4,6},{5,3},{6,4},{7,1},{8,10},{9,15},{10,... | collective-permute-start | bytes 1572872 | tf_op jit(solution)/shard_map/ppermute | solution.py:33
  105.0 21.9 %collective-permute-start.20 = (bf16[128,2048]{1,0:T(8,128)(2,1)S(1)}, bf16[128,2048]{1,0:T(8,128)(2,1)S(1)}, u32[]{:S(2)}, u32[]{:S(2)}) collective-permute-start(bf16[128,2048]{1,0:T(8,128)(2,1)S(1)} %shard_map.73), channel_id=1, source_target_pairs={{0,2},{1,7},{2,0},{3,5},{4,6},{5,3},{6,4},{7,1},{8,10},{9,15},{10,... | collective-permute-start | bytes 1572872 | tf_op jit(solution)/shard_map/ppermute | solution.py:33
  107.1 29.0 %collective-permute-start.17 = (bf16[128,2048]{1,0:T(8,128)(2,1)S(1)}, bf16[128,2048]{1,0:T(8,128)(2,1)S(1)}, u32[]{:S(2)}, u32[]{:S(2)}) collective-permute-start(bf16[128,2048]{1,0:T(8,128)(2,1)S(1)} %shard_map.70), channel_id=1, source_target_pairs={{0,2},{1,7},{2,0},{3,5},{4,6},{5,3},{6,4},{7,1},{8,10},{9,15},{10,... | collective-permute-start | bytes 1572872 | tf_op jit(solution)/shard_map/ppermute | solution.py:33
  113.3 27.7 %collective-permute-start.24 = (bf16[64,2048]{1,0:T(8,128)(2,1)S(1)}, bf16[64,2048]{1,0:T(8,128)(2,1)S(1)}, u32[]{:S(2)}, u32[]{:S(2)}) collective-permute-start(bf16[64,2048]{1,0:T(8,128)(2,1)S(1)} %shard_map.77), channel_id=1, source_target_pairs={{0,6},{1,3},{2,4},{3,1},{4,2},{5,7},{6,0},{7,5},{8,14},{9,11},{10,... | collective-permute-start | bytes 786440 | tf_op jit(solution)/shard_map/ppermute | solution.py:33
  117.1 22.5 %collective-permute-start.27 = (bf16[64,2048]{1,0:T(8,128)(2,1)S(1)}, bf16[64,2048]{1,0:T(8,128)(2,1)S(1)}, u32[]{:S(2)}, u32[]{:S(2)}) collective-permute-start(bf16[64,2048]{1,0:T(8,128)(2,1)S(1)} %shard_map.80), channel_id=1, source_target_pairs={{0,6},{1,3},{2,4},{3,1},{4,2},{5,7},{6,0},{7,5},{8,14},{9,11},{10,... | collective-permute-start | bytes 786440 | tf_op jit(solution)/shard_map/ppermute | solution.py:33
  127.5 14.8 %collective-permute-start.21 = (bf16[64,2048]{1,0:T(8,128)(2,1)S(1)}, bf16[64,2048]{1,0:T(8,128)(2,1)S(1)}, u32[]{:S(2)}, u32[]{:S(2)}) collective-permute-start(bf16[64,2048]{1,0:T(8,128)(2,1)S(1)} %shard_map.74), channel_id=1, source_target_pairs={{0,6},{1,3},{2,4},{3,1},{4,2},{5,7},{6,0},{7,5},{8,14},{9,11},{10,... | collective-permute-start | bytes 786440 | tf_op jit(solution)/shard_map/ppermute | solution.py:33
  136.8 7.7 %collective-permute-start.18 = (bf16[64,2048]{1,0:T(8,128)(2,1)S(1)}, bf16[64,2048]{1,0:T(8,128)(2,1)S(1)}, u32[]{:S(2)}, u32[]{:S(2)}) collective-permute-start(bf16[64,2048]{1,0:T(8,128)(2,1)S(1)} %shard_map.71), channel_id=1, source_target_pairs={{0,6},{1,3},{2,4},{3,1},{4,2},{5,7},{6,0},{7,5},{8,14},{9,11},{10,... | collective-permute-start | bytes 786440 | tf_op jit(solution)/shard_map/ppermute | solution.py:33

commit v2 on v1

v2 whole, which is shorter than its diff:
```python
import functools

import jax
import jax.numpy as jnp
from jax import lax
from jax.experimental import pallas as pl
from jax.experimental.pallas import tpu as pltpu
from jax.sharding import Mesh, PartitionSpec as P


D = 2048
LANES = 128
WIDTH = 704
ROWS = 256
CHUNKS = ((0, 48), (48, 112), (160, 64), (224, 32))
VMEM = pl.BlockSpec(memory_space=pltpu.VMEM)
SMEM = pl.BlockSpec(memory_space=pltpu.SMEM)
ANY = pl.BlockSpec(memory_space=pl.ANY)


def call(kernel, out, mib, **kw):
    return pl.pallas_call(kernel, out_shape=out, compiler_params=pltpu.CompilerParams(vmem_limit_bytes=mib << 20), **kw)


def masks(core):
    return (1, 3) if core == 0 else (3, 1)


def pair_up(value, axis, step):
    pairs = [(i * 2 + c, (i ^ masks(c)[step]) * 2 + c) for i in range(4) for c in range(2)]
    return lax.ppermute(value, (axis, "c"), pairs)


def double(block, route):
    have = block[None]
    for n, (axis, step) in enumerate(route):
        other = pair_up(have, axis, step)
        if n == 3:
            return have, other
        have = jnp.concatenate([have, other], axis=0)


def place_of(route, k, pos):
    at = {"z": pos[0], "y": pos[1]}
    m = (1 + 2 * pos[3], 3 - 2 * pos[3])
    for n, (axis, step) in enumerate(route):
        if (k >> n) & 1:
            at[axis] = at[axis] ^ m[step]
    return at["z"] * 4 + at["y"]


def token_block(p, pos):
    core = jnp.where(p < 4, 1 - pos[3], pos[3])
    q = p & 3
    mask = jnp.where(q == 0, 2, jnp.where(q == 1, 1 + 2 * core, jnp.where(q == 2, 3 - 2 * core, 0)))
    return (pos[2] ^ mask) * 2 + core


ZZYY = (("z", 0), ("z", 1), ("y", 0), ("y", 1))
YYZZ = (("y", 0), ("y", 1), ("z", 0), ("z", 1))
ZYZY = (("z", 0), ("y", 0), ("z", 1), ("y", 1))
YZYZ = (("y", 0), ("z", 0), ("y", 1), ("z", 1))


def scale_kernel(x_ref, out_ref):
    for i in range(0, x_ref.shape[0], ROWS):
        xf = x_ref[i:i + ROWS].astype(jnp.float32)
        scale = lax.rsqrt(jnp.mean(xf * xf, axis=-1, keepdims=True) + 1e-06)
        out_ref[i:i + ROWS] = jnp.broadcast_to(scale, (ROWS, LANES))


def scales(tokens):
    return call(
        scale_kernel, jax.ShapeDtypeStruct((tokens.shape[0], LANES), jnp.float32), 12,
        in_specs=[VMEM], out_specs=VMEM,
    )(tokens)


def place_kernel(first, routes, pos, *refs):
    out_ref = refs[-1]
    height = WIDTH // len(routes)
    for n, route in enumerate(routes):
        for k in range(8):
            at = pl.multiple_of(place_of(route, first + k, pos) * LANES, LANES)
            out_ref[n * height:(n + 1) * height, pl.ds(at, LANES)] = refs[n][k]


def place(pos, routes, halves, first, into):
    shape = jax.ShapeDtypeStruct((WIDTH, D), jnp.bfloat16)
    more = [] if into is None else [into]
    return call(
        functools.partial(place_kernel, first, routes), shape, 8,
        in_specs=[SMEM] + [VMEM] * (len(halves) + len(more)), out_specs=VMEM,
        input_output_aliases={1 + len(halves): 0} if more else {},
    )(pos, *halves, *more)


def nt(left, right):
    return lax.dot_general(left, right, (((1,), (1,)), ((), ())), preferred_element_type=jnp.float32)


def hidden_kernel(skip, pos, xa_ref, xb_ref, gate_ref, up_ref, scale_ref, out_ref):
    at = pl.program_id(0) * 2 + skip
    x = jnp.concatenate([xa_ref[...], xb_ref[...]], axis=0)
    rows = [pl.ds(pl.multiple_of(token_block(at + i, pos) * ROWS, ROWS), ROWS) for i in range(2)]
    scale = jnp.concatenate([scale_ref[r, :] for r in rows], axis=0)[:, :1]
    gate = nt(x, gate_ref[...]) * scale
    up = nt(x, up_ref[...]) * scale
    hidden = (gate / (1.0 + jnp.exp(-gate)) * up).astype(jnp.bfloat16)
    out_ref[...] = hidden.reshape(out_ref.shape)


def hidden_of(pos, skip, count, tokens, gate, up, scale):
    return call(
        functools.partial(hidden_kernel, skip), jax.ShapeDtypeStruct((count, ROWS, WIDTH), jnp.bfloat16), 20,
        grid_spec=pltpu.PrefetchScalarGridSpec(
            num_scalar_prefetch=1,
            grid=(count // 2,),
            in_specs=[
                pl.BlockSpec((ROWS, D), lambda i, pos: (token_block(2 * i + skip, pos), 0)),
                pl.BlockSpec((ROWS, D), lambda i, pos: (token_block(2 * i + skip + 1, pos), 0)),
                VMEM, VMEM, VMEM,
            ],
            out_specs=pl.BlockSpec((2, ROWS, WIDTH), lambda i, pos: (i, 0, 0)),
        ),
    )(pos, tokens, tokens, gate, up, scale)


def down_kernel(rows, picks, at, split, *refs):
    n_hidden = max(i for i, _ in picks) + 1
    hidden, down_ref, refs = refs[:n_hidden], refs[n_hidden], refs[n_hidden + 1:]
    more, outs = refs[:len(at)], refs[len(at):]
    size = rows.stop - rows.start
    h = jnp.concatenate([hidden[i][j, rows, :] for i, j in picks], axis=0)
    for n in range(0, D, 512):
        part = jnp.dot(h, down_ref[:, n:n + 512], preferred_element_type=jnp.float32)
        for ref, start in zip(more, at):
            part = part + ref[start * size:start * size + h.shape[0], n:n + 512].astype(jnp.float32)
        outs[0][:, n:n + 512] = (part[:size] if split else part).astype(jnp.bfloat16)
        if split:
            outs[1][:, n:n + 512] = part[size:]


def down_of(chunk, hidden, picks, down, more, split=False):
    start, size = chunk
    kernel = functools.partial(down_kernel, slice(start, start + size), picks, [m[1] for m in more], split)
    ins = [*hidden, down, *[m[0] for m in more]]
    if split:
        out = [jax.ShapeDtypeStruct((size, D), t) for t in (jnp.bfloat16, jnp.float32)]
    else:
        out = jax.ShapeDtypeStruct((len(picks) * size, D), jnp.bfloat16)
    return call(kernel, out, 12, in_specs=[VMEM] * len(ins), out_specs=[VMEM] * 2 if split else VMEM)(*ins)


def last_kernel(rows, own_ref, got_ref, *refs):
    out_ref, buf, sem = refs[-3:]
    buf[...] = (own_ref[...] + got_ref[...].astype(jnp.float32)).astype(jnp.bfloat16)
    copy = pltpu.make_async_copy(buf, out_ref.at[rows], sem)
    copy.start()
    copy.wait()


def last_of(chunk, own, got, into):
    start, size = chunk
    more = [] if into is None else [into]
    return call(
        functools.partial(last_kernel, slice(start, start + size)), jax.ShapeDtypeStruct((ROWS, D), jnp.bfloat16), 8,
        in_specs=[VMEM] * 2 + [ANY] * len(more), out_specs=ANY,
        scratch_shapes=[pltpu.VMEM((size, D), jnp.bfloat16), pltpu.SemaphoreType.DMA],
        input_output_aliases={2: 0} if more else {},
    )(own, got, *more)


def per_device(tokens, norm_gain, gate_weight, up_weight, down_weight):
    z, y, x, c = (lax.axis_index(a) for a in "zyxc")
    k = jnp.arange(4, dtype=jnp.int32)
    pos = jnp.where(k == 0, z, jnp.where(k == 1, y, jnp.where(k == 2, x, c)))
    half = WIDTH // 2
    blocks = [gate_weight.T, up_weight.T, down_weight[:half], down_weight[half:]]
    gain = lax.dynamic_slice(norm_gain, ((z * 4 + y) * LANES,), (LANES,))
    for i in range(2):
        blocks[i] = (blocks[i].astype(jnp.float32) * gain).astype(jnp.bfloat16)
    blocks[0], blocks[1], pos = lax.optimization_barrier((blocks[0], blocks[1], pos))
    gate = double(blocks[0], ZZYY)
    up = double(blocks[1], YYZZ)
    down = [double(blocks[2], ZYZY), double(blocks[3], YZYZ)]

    scale = scales(tokens)
    gw = place(pos, [ZZYY], gate[:1], 0, None)
    gw = place(pos, [ZZYY], gate[1:], 8, gw)
    uw = place(pos, [YYZZ], up[:1], 0, None)
    uw = place(pos, [YYZZ], up[1:], 8, uw)
    hid = [hidden_of(pos, n, m, tokens, gw, uw, scale) for n, m in ((0, 2), (2, 6))]
    dw = place(pos, [ZYZY, YZYZ], [d[0] for d in down], 0, None)
    dw = place(pos, [ZYZY, YZYZ], [d[1] for d in down], 8, dw)

    out = None
    for chunk in CHUNKS:
        sent = down_of(chunk, hid, [(0, 0), (0, 1), (1, 0), (1, 1)], dw, [])
        got = lax.ppermute(sent, "c", [(0, 1), (1, 0)])
        sent = down_of(chunk, hid[1:], [(0, 2), (0, 3)], dw, [(got, 0)])
        got1 = pair_up(sent, "x", 0)
        sent, own = down_of(chunk, hid[1:], [(0, 4), (0, 5)], dw, [(got, 2), (got1, 0)], True)
        got2 = pair_up(sent, "x", 1)
        out = last_of(chunk, own, got2, out)
    return out


def solution(mesh):
    torus = Mesh(mesh.devices.reshape(4, 4, 4, 2), ("z", "y", "x", "c"))
    fs, tp = ("z", "y"), ("x", "c")
    placed = (P(fs, None), P(), P(fs, tp), P(fs, tp), P(tp, fs))
    return jax.shard_map(per_device, mesh=torus, in_specs=placed, out_specs=P(fs + tp, None), check_vma=False)
```

time: 146 us -> 142 us (0.973)
  the two profiles are of different devices: /device:TPU:0 before, /device:TPU:1 now
where the time goes in v2:
time: 142 us; the launch traced here: 140 us
  waiting for transfers between devices  62.4 us (44%)
  starting transfers between devices  39 us (27%)
  Pallas kernels  35.1 us (25%)
  other arithmetic  1.85 us (1%)
    ppermute x24, waiting for transfers between devices, pair_up(): return lax.ppermute(value, (axis, 'c'), pairs)  61.6 us
    ppermute x24, starting transfers between devices, pair_up(): return lax.ppermute(value, (axis, 'c'), pairs)  30.7 us
    pallas_call x2, Pallas kernels, hidden_of(): call(functools.partial(hidden_kernel, skip), jax.ShapeDtypeStruct((count,...  15 us
    pallas_call x12, Pallas kernels, down_of(): call(kernel, out, 12, in_specs=[VMEM] * len(ins), out_specs=[VMEM] * 2 if...  9.51 us
    ppermute x4, starting transfers between devices, per_device(): got = lax.ppermute(sent, 'c', [(0, 1), (1, 0)])  8.23 us
    pallas_call x6, Pallas kernels, place(): call(functools.partial(place_kernel, first, routes), shape, 8, in_specs=[...  5.75 us
    pallas_call x4, Pallas kernels, last_of(): call(functools.partial(last_kernel, slice(start, start + size)), jax.Shap...  3.03 us
  transfers between devices with their start and end apart: 28, of which 15 were waited for; matrix products, arithmetic and copies ran while one was open for 1% of the time, Pallas kernels for 12%

profile of v2, /device:TPU:1, one launch (start us, length us, event | category | flops | bytes accessed | tf_op | source)
XLA Modules:
  0.0 139.6 jit_solution(8289630579651742425)
XLA Ops:
  0.0 0.8 dynamic_slice.3
  0.8 1.1 fusion.1
  1.8 3.6 %collective-permute-start.4 = (bf16[1,704,128]{2,1,0:T(8,128)(2,1)S(1)}, bf16[1,704,128]{2,1,0:T(8,128)(2,1)S(1)}, u32[]{:S(2)}, u32[]{:S(2)}) collective-permute-start(bf16[1,704,128]{2,1,0:T(8,128)(2,1)S(1)} %bitcast.16), channel_id=1, source_target_pairs={{0,8},{1,25},{8,0},{9,17},{16,24},{17,9},{24,16},{25,1},{2,10},{3,... | collective-permute-start | bytes 540680 | tf_op jit(solution)/shard_map/ppermute | solution.py:31
  5.5 3.8 %collective-permute-start = (bf16[1,704,128]{2,1,0:T(8,128)(2,1)S(1)}, bf16[1,704,128]{2,1,0:T(8,128)(2,1)S(1)}, u32[]{:S(2)}, u32[]{:S(2)}) collective-permute-start(bf16[1,704,128]{2,1,0:T(8,128)(2,1)S(1)} %bitcast.12), channel_id=1, source_target_pairs={{0,32},{1,97},{32,0},{33,65},{64,96},{65,33},{96,64},{97,1},{2,34}... | collective-permute-start | bytes 540680 | tf_op jit(solution)/shard_map/ppermute | solution.py:31
  9.4 2.7 %collective-permute-done = bf16[1,704,128]{2,1,0:T(8,128)(2,1)S(1)} collective-permute-done((bf16[1,704,128]{2,1,0:T(8,128)(2,1)S(1)}, bf16[1,704,128]{2,1,0:T(8,128)(2,1)S(1)}, u32[]{:S(2)}, u32[]{:S(2)}) %collective-permute-start) | collective-permute-done | bytes 180256 | tf_op jit(solution)/shard_map/ppermute | solution.py:31
  12.2 0.1 collective-permute-start.1
  12.3 3.7 %collective-permute-done.5 = bf16[2,704,128]{2,1,0:T(8,128)(2,1)S(1)} collective-permute-done((bf16[2,704,128]{2,1,0:T(8,128)(2,1)S(1)}, bf16[2,704,128]{2,1,0:T(8,128)(2,1)S(1)}, u32[]{:S(2)}, u32[]{:S(2)}) %collective-permute-start.5) | collective-permute-done | bytes 360480 | tf_op jit(solution)/shard_map/ppermute | solution.py:31
  16.0 3.0 %collective-permute-start.6 = (bf16[4,704,128]{2,1,0:T(8,128)(2,1)S(1)}, bf16[4,704,128]{2,1,0:T(8,128)(2,1)S(1)}, u32[]{:S(2)}, u32[]{:S(2)}) collective-permute-start(bf16[4,704,128]{2,1,0:T(8,128)(2,1)S(1)} %pad_maximum_fusion.3), channel_id=1, source_target_pairs={{0,32},{1,97},{32,0},{33,65},{64,96},{65,33},{96,64},{97,1},{2,34}... | collective-permute-start | bytes 2162696 | tf_op jit(solution)/shard_map/ppermute | solution.py:31
  19.0 2.8 %collective-permute-start.2 = (bf16[4,704,128]{2,1,0:T(8,128)(2,1)S(1)}, bf16[4,704,128]{2,1,0:T(8,128)(2,1)S(1)}, u32[]{:S(2)}, u32[]{:S(2)}) collective-permute-start(bf16[4,704,128]{2,1,0:T(8,128)(2,1)S(1)} %pad_maximum_fusion.2), channel_id=1, source_target_pairs={{0,8},{1,25},{8,0},{9,17},{16,24},{17,9},{24,16},{25,1},{2,10},{3,... | collective-permute-start | bytes 2162696 | tf_op jit(solution)/shard_map/ppermute | solution.py:31
  21.8 0.1 collective-permute-start.8
  21.9 2.5 %collective-permute-start.12 = (bf16[1,352,128]{2,1,0:T(8,128)(2,1)S(1)}, bf16[1,352,128]{2,1,0:T(8,128)(2,1)S(1)}, u32[]{:S(2)}, u32[]{:S(2)}) collective-permute-start(bf16[1,352,128]{2,1,0:T(8,128)(2,1)S(1)} %get-tuple-element.27), channel_id=1, source_target_pairs={{0,8},{1,25},{8,0},{9,17},{16,24},{17,9},{24,16},{25,1},{2,10},{3,... | collective-permute-start | bytes 270344 | tf_op jit(solution)/shard_map/ppermute | solution.py:31
  24.4 5.2 %collective-permute-done.8 = bf16[1,352,128]{2,1,0:T(8,128)(2,1)S(1)} collective-permute-done((bf16[1,352,128]{2,1,0:T(8,128)(2,1)S(1)}, bf16[1,352,128]{2,1,0:T(8,128)(2,1)S(1)}, u32[]{:S(2)}, u32[]{:S(2)}) %collective-permute-start.8) | collective-permute-done | bytes 90144 | tf_op jit(solution)/shard_map/ppermute | solution.py:31
  29.6 1.7 %collective-permute-start.9 = (bf16[2,352,128]{2,1,0:T(8,128)(2,1)S(1)}, bf16[2,352,128]{2,1,0:T(8,128)(2,1)S(1)}, u32[]{:S(2)}, u32[]{:S(2)}) collective-permute-start(bf16[2,352,128]{2,1,0:T(8,128)(2,1)S(1)} %pad_maximum_fusion.10), channel_id=1, source_target_pairs={{0,8},{1,25},{8,0},{9,17},{16,24},{17,9},{24,16},{25,1},{2,10},{3,... | collective-permute-start | bytes 540680 | tf_op jit(solution)/shard_map/ppermute | solution.py:31
  31.5 2.7 %collective-permute-start.13 = (bf16[2,352,128]{2,1,0:T(8,128)(2,1)S(1)}, bf16[2,352,128]{2,1,0:T(8,128)(2,1)S(1)}, u32[]{:S(2)}, u32[]{:S(2)}) collective-permute-start(bf16[2,352,128]{2,1,0:T(8,128)(2,1)S(1)} %pad_maximum_fusion.11), channel_id=1, source_target_pairs={{0,32},{1,97},{32,0},{33,65},{64,96},{65,33},{96,64},{97,1},{2,34}... | collective-permute-start | bytes 540680 | tf_op jit(solution)/shard_map/ppermute | solution.py:31
  34.2 0.1 pad_maximum_fusion.1.refs_0_
  34.3 0.1 collective-permute-start.7
  34.4 0.1 pad_maximum_fusion.refs_0_
  34.7 0.6 collective-permute-done.9
  35.3 0.9 collective-permute-start.10
  36.3 0.9 collective-permute-done.13
  37.2 0.7 collective-permute-start.14
  37.8 20.5 %collective-permute-done.10 = bf16[4,352,128]{2,1,0:T(8,128)(2,1)S(1)} collective-permute-done((bf16[4,352,128]{2,1,0:T(8,128)(2,1)S(1)}, bf16[4,352,128]{2,1,0:T(8,128)(2,1)S(1)}, u32[]{:S(2)}, u32[]{:S(2)}) %collective-permute-start.10) | collective-permute-done | bytes 360480 | tf_op jit(solution)/shard_map/ppermute | solution.py:31
  58.6 0.3 collective-permute-start.15
  58.9 1.7 %shard_map.59.scale_ref = f32[2048,128]{1,0:T(8,128)S(1)} custom-call(bf16[2048,2048]{1,0:T(8,128)(2,1)S(1)} %bitcast.11), custom_call_target="tpu_custom_call" | custom-call | tf_op jit(solution)/shard_map/pallas_call | solution.py:73
  60.7 1.0 shard_map.61.refs_2_
  61.6 1.0 shard_map.57.refs_1_
  62.6 1.0 shard_map.55.refs_1_
  63.6 5.4 %collective-permute-done.11.refs_0_ = bf16[8,352,128]{2,1,0:T(8,128)(2,1)S(1)} collective-permute-done((bf16[8,352,128]{2,1,0:T(8,128)(2,1)S(1)}, bf16[8,352,128]{2,1,0:T(8,128)(2,1)S(1)}, u32[]{:S(2)}, u32[]{:S(2)}) %collective-permute-start.11) | collective-permute-done | bytes 720928 | tf_op jit(solution)/shard_map/ppermute | solution.py:31
  68.9 0.4 collective-permute-done.15.refs_1_
  69.3 0.9 shard_map.62.refs_2_.refs_1_
  70.3 1.0 shard_map.58.up_ref
  71.3 1.0 shard_map.56.gate_ref
  72.2 4.0 %shard_map.63.refs_0_ = bf16[2,256,704]{2,1,0:T(8,128)(2,1)S(1)} custom-call(s32[4]{0:T(128)S(1)} %compare_select_fusion.2.pos, bf16[2048,2048]{1,0:T(8,128)(2,1)S(1)} %bitcast.11, bf16[2048,2048]{1,0:T(8,128)(2,1)S(1)} %bitcast.11, bf16[704,2048]{1,0:T(8,128)(2,1)S(1)} %shard_map.56.gate_ref, bf16[704,2048]{1,0:T(8,128)(2,1)S(1)} %shard_map.58.up_ref, ...), custom_call_target="tpu_custom_call" | custom-call | tf_op jit(solution)/shard_map/pallas_call | solution.py:114
  76.2 11.0 %shard_map.60.refs_1_.refs_0_ = bf16[6,256,704]{2,1,0:T(8,128)(2,1)S(1)} custom-call(s32[4]{0:T(128)S(1)} %compare_select_fusion.2.pos, bf16[2048,2048]{1,0:T(8,128)(2,1)S(1)} %bitcast.11, bf16[2048,2048]{1,0:T(8,128)(2,1)S(1)} %bitcast.11, bf16[704,2048]{1,0:T(8,128)(2,1)S(1)} %shard_map.56.gate_ref, bf16[704,2048]{1,0:T(8,128)(2,1)S(1)} %shard_map.58.up_ref, ...), custom_call_target="tpu_custom_call" | custom-call | tf_op jit(solution)/shard_map/pallas_call | solution.py:114
  87.3 1.6 %shard_map.70 = bf16[448,2048]{1,0:T(8,128)(2,1)S(1)} custom-call(bf16[2,256,704]{2,1,0:T(8,128)(2,1)S(1)} %shard_map.63.refs_0_, bf16[6,256,704]{2,1,0:T(8,128)(2,1)S(1)} %shard_map.60.refs_1_.refs_0_, bf16[704,2048]{1,0:T(8,128)(2,1)S(1)} %shard_map.62.refs_2_.refs_1_), custom_call_target="tpu_custom_call" | custom-call | tf_op jit(solution)/shard_map/pallas_call | solution.py:152
  88.9 7.3 %collective-permute-start.22 = (bf16[448,2048]{1,0:T(8,128)(2,1)S(1)}, bf16[448,2048]{1,0:T(8,128)(2,1)S(1)}, u32[]{:S(2)}, u32[]{:S(2)}) collective-permute-start(bf16[448,2048]{1,0:T(8,128)(2,1)S(1)} %shard_map.70), channel_id=1, source_target_pairs={{0,1},{1,0},{2,3},{3,2},{4,5},{5,4},{6,7},{7,6},{8,9},{9,8},{10,11... | collective-permute-start | bytes 5505032 | tf_op jit(solution)/shard_map/ppermute | solution.py:200
  96.1 1.0 shard_map.67
  97.1 0.1 collective-permute-start.19
  97.2 0.8 shard_map.73
  98.0 0.8 collective-permute-start.25
  98.8 0.7 collective-permute-done.22.refs_2_
  99.5 0.9 shard_map.71
  100.4 2.6 %collective-permute-start.23 = (bf16[224,2048]{1,0:T(8,128)(2,1)S(1)}, bf16[224,2048]{1,0:T(8,128)(2,1)S(1)}, u32[]{:S(2)}, u32[]{:S(2)}) collective-permute-start(bf16[224,2048]{1,0:T(8,128)(2,1)S(1)} %shard_map.71), channel_id=1, source_target_pairs={{0,2},{1,7},{2,0},{3,5},{4,6},{5,3},{6,4},{7,1},{8,10},{9,15},{10,... | collective-permute-start | bytes 2752520 | tf_op jit(solution)/shard_map/ppermute | solution.py:31
  103.0 0.6 shard_map.64
  103.7 0.6 shard_map.68
  104.3 1.3 collective-permute-start.20
  105.6 0.6 shard_map.74
  106.2 1.6 %collective-permute-start.26 = (bf16[96,2048]{1,0:T(8,128)(2,1)S(1)}, bf16[96,2048]{1,0:T(8,128)(2,1)S(1)}, u32[]{:S(2)}, u32[]{:S(2)}) collective-permute-start(bf16[96,2048]{1,0:T(8,128)(2,1)S(1)} %shard_map.74), channel_id=1, source_target_pairs={{0,2},{1,7},{2,0},{3,5},{4,6},{5,3},{6,4},{7,1},{8,10},{9,15},{10,... | collective-permute-start | bytes 1179656 | tf_op jit(solution)/shard_map/ppermute | solution.py:31
  107.7 6.2 %collective-permute-done.23.refs_3_ = bf16[224,2048]{1,0:T(8,128)(2,1)S(1)} collective-permute-done((bf16[224,2048]{1,0:T(8,128)(2,1)S(1)}, bf16[224,2048]{1,0:T(8,128)(2,1)S(1)}, u32[]{:S(2)}, u32[]{:S(2)}) %collective-permute-start.23) | collective-permute-done | bytes 917536 | tf_op jit(solution)/shard_map/ppermute | solution.py:31
  114.0 0.9 shard_map.72
  114.9 0.4 collective-permute-start.24
  115.3 0.6 shard_map.65
  115.9 2.3 %collective-permute-start.17 = (bf16[64,2048]{1,0:T(8,128)(2,1)S(1)}, bf16[64,2048]{1,0:T(8,128)(2,1)S(1)}, u32[]{:S(2)}, u32[]{:S(2)}) collective-permute-start(bf16[64,2048]{1,0:T(8,128)(2,1)S(1)} %shard_map.65), channel_id=1, source_target_pairs={{0,2},{1,7},{2,0},{3,5},{4,6},{5,3},{6,4},{7,1},{8,10},{9,15},{10,... | collective-permute-start | bytes 786440 | tf_op jit(solution)/shard_map/ppermute | solution.py:31
  118.2 1.8 %collective-permute-done.20.refs_3_ = bf16[128,2048]{1,0:T(8,128)(2,1)S(1)} collective-permute-done((bf16[128,2048]{1,0:T(8,128)(2,1)S(1)}, bf16[128,2048]{1,0:T(8,128)(2,1)S(1)}, u32[]{:S(2)}, u32[]{:S(2)}) %collective-permute-start.20) | collective-permute-done | bytes 524320 | tf_op jit(solution)/shard_map/ppermute | solution.py:31
  120.1 0.6 shard_map.69
  120.8 7.7 %collective-permute-done.26.refs_3_ = bf16[96,2048]{1,0:T(8,128)(2,1)S(1)} collective-permute-done((bf16[96,2048]{1,0:T(8,128)(2,1)S(1)}, bf16[96,2048]{1,0:T(8,128)(2,1)S(1)}, u32[]{:S(2)}, u32[]{:S(2)}) %collective-permute-start.26) | collective-permute-done | bytes 393248 | tf_op jit(solution)/shard_map/ppermute | solution.py:31
  128.5 0.6 shard_map.75
  129.2 4.9 %collective-permute-done.17.refs_3_ = bf16[64,2048]{1,0:T(8,128)(2,1)S(1)} collective-permute-done((bf16[64,2048]{1,0:T(8,128)(2,1)S(1)}, bf16[64,2048]{1,0:T(8,128)(2,1)S(1)}, u32[]{:S(2)}, u32[]{:S(2)}) %collective-permute-start.17) | collective-permute-done | bytes 262176 | tf_op jit(solution)/shard_map/ppermute | solution.py:31
  134.1 0.6 shard_map.66
  134.9 1.5 %collective-permute-done.27.got_ref = bf16[48,2048]{1,0:T(8,128)(2,1)S(1)} collective-permute-done((bf16[48,2048]{1,0:T(8,128)(2,1)S(1)}, bf16[48,2048]{1,0:T(8,128)(2,1)S(1)}, u32[]{:S(2)}, u32[]{:S(2)}) %collective-permute-start.27) | collective-permute-done | bytes 196640 | tf_op jit(solution)/shard_map/ppermute | solution.py:31
  136.4 0.7 shard_map.76.refs_0_
  137.1 0.9 shard_map.77.refs_0_
  138.0 0.8 shard_map.78.refs_0_
  138.8 0.7 shard_map.79
  (40 shorter events, 1.2 us)
Async XLA Ops:
  1.8 7.4 %collective-permute-start.4 = (bf16[1,704,128]{2,1,0:T(8,128)(2,1)S(1)}, bf16[1,704,128]{2,1,0:T(8,128)(2,1)S(1)}, u32[]{:S(2)}, u32[]{:S(2)}) collective-permute-start(bf16[1,704,128]{2,1,0:T(8,128)(2,1)S(1)} %bitcast.16), channel_id=1, source_target_pairs={{0,8},{1,25},{8,0},{9,17},{16,24},{17,9},{24,16},{25,1},{2,10},{3,... | collective-permute-start | bytes 540680 | tf_op jit(solution)/shard_map/ppermute | solution.py:31
  5.5 6.6 %collective-permute-start = (bf16[1,704,128]{2,1,0:T(8,128)(2,1)S(1)}, bf16[1,704,128]{2,1,0:T(8,128)(2,1)S(1)}, u32[]{:S(2)}, u32[]{:S(2)}) collective-permute-start(bf16[1,704,128]{2,1,0:T(8,128)(2,1)S(1)} %bitcast.12), channel_id=1, source_target_pairs={{0,32},{1,97},{32,0},{33,65},{64,96},{65,33},{96,64},{97,1},{2,34}... | collective-permute-start | bytes 540680 | tf_op jit(solution)/shard_map/ppermute | solution.py:31
  9.2 12.6 %copy-start = (bf16[704,128]{1,0:T(8,128)(2,1)S(1)}, bf16[704,128]{1,0:T(8,128)(2,1)}, u32[]{:S(2)}) copy-start(bf16[704,128]{1,0:T(8,128)(2,1)} %param.9) | copy-start | bytes 540676
  9.2 49.7 %slice-start = ((s8[8388608]{0:T(1024)(128)(4,1)}), s8[4194304]{0:T(1024)(128)(4,1)S(1)}, s32[]{:S(2)}) async-start(s8[8388608]{0:T(1024)(128)(4,1)} %bitcast.10), calls=%async_computation | async-start | bytes 8388608
  9.3 6.7 %collective-permute-start.5 = (bf16[2,704,128]{2,1,0:T(8,128)(2,1)S(1)}, bf16[2,704,128]{2,1,0:T(8,128)(2,1)S(1)}, u32[]{:S(2)}, u32[]{:S(2)}) collective-permute-start(bf16[2,704,128]{2,1,0:T(8,128)(2,1)S(1)} %pad_maximum_fusion.7), channel_id=1, source_target_pairs={{0,24},{1,9},{8,16},{9,1},{16,8},{17,25},{24,0},{25,17},{2,26},{3,... | collective-permute-start | bytes 1081352 | tf_op jit(solution)/shard_map/ppermute | solution.py:31
  12.2 6.8 %collective-permute-start.1 = (bf16[2,704,128]{2,1,0:T(8,128)(2,1)S(1)}, bf16[2,704,128]{2,1,0:T(8,128)(2,1)S(1)}, u32[]{:S(2)}, u32[]{:S(2)}) collective-permute-start(bf16[2,704,128]{2,1,0:T(8,128)(2,1)S(1)} %pad_maximum_fusion.6), channel_id=1, source_target_pairs={{0,96},{1,33},{32,64},{33,1},{64,32},{65,97},{96,0},{97,65},{2,98}... | collective-permute-start | bytes 1081352 | tf_op jit(solution)/shard_map/ppermute | solution.py:31
  16.0 18.2 %collective-permute-start.6 = (bf16[4,704,128]{2,1,0:T(8,128)(2,1)S(1)}, bf16[4,704,128]{2,1,0:T(8,128)(2,1)S(1)}, u32[]{:S(2)}, u32[]{:S(2)}) collective-permute-start(bf16[4,704,128]{2,1,0:T(8,128)(2,1)S(1)} %pad_maximum_fusion.3), channel_id=1, source_target_pairs={{0,32},{1,97},{32,0},{33,65},{64,96},{65,33},{96,64},{97,1},{2,34}... | collective-permute-start | bytes 2162696 | tf_op jit(solution)/shard_map/ppermute | solution.py:31
  19.0 15.4 %collective-permute-start.2 = (bf16[4,704,128]{2,1,0:T(8,128)(2,1)S(1)}, bf16[4,704,128]{2,1,0:T(8,128)(2,1)S(1)}, u32[]{:S(2)}, u32[]{:S(2)}) collective-permute-start(bf16[4,704,128]{2,1,0:T(8,128)(2,1)S(1)} %pad_maximum_fusion.2), channel_id=1, source_target_pairs={{0,8},{1,25},{8,0},{9,17},{16,24},{17,9},{24,16},{25,1},{2,10},{3,... | collective-permute-start | bytes 2162696 | tf_op jit(solution)/shard_map/ppermute | solution.py:31
  21.8 7.8 %collective-permute-start.8 = (bf16[1,352,128]{2,1,0:T(8,128)(2,1)S(1)}, bf16[1,352,128]{2,1,0:T(8,128)(2,1)S(1)}, u32[]{:S(2)}, u32[]{:S(2)}) collective-permute-start(bf16[1,352,128]{2,1,0:T(8,128)(2,1)S(1)} %get-tuple-element.28), channel_id=1, source_target_pairs={{0,32},{1,97},{32,0},{33,65},{64,96},{65,33},{96,64},{97,1},{2,34}... | collective-permute-start | bytes 270344 | tf_op jit(solution)/shard_map/ppermute | solution.py:31
  21.9 9.5 %collective-permute-start.12 = (bf16[1,352,128]{2,1,0:T(8,128)(2,1)S(1)}, bf16[1,352,128]{2,1,0:T(8,128)(2,1)S(1)}, u32[]{:S(2)}, u32[]{:S(2)}) collective-permute-start(bf16[1,352,128]{2,1,0:T(8,128)(2,1)S(1)} %get-tuple-element.27), channel_id=1, source_target_pairs={{0,8},{1,25},{8,0},{9,17},{16,24},{17,9},{24,16},{25,1},{2,10},{3,... | collective-permute-start | bytes 270344 | tf_op jit(solution)/shard_map/ppermute | solution.py:31
  29.6 5.6 %collective-permute-start.9 = (bf16[2,352,128]{2,1,0:T(8,128)(2,1)S(1)}, bf16[2,352,128]{2,1,0:T(8,128)(2,1)S(1)}, u32[]{:S(2)}, u32[]{:S(2)}) collective-permute-start(bf16[2,352,128]{2,1,0:T(8,128)(2,1)S(1)} %pad_maximum_fusion.10), channel_id=1, source_target_pairs={{0,8},{1,25},{8,0},{9,17},{16,24},{17,9},{24,16},{25,1},{2,10},{3,... | collective-permute-start | bytes 540680 | tf_op jit(solution)/shard_map/ppermute | solution.py:31
  31.5 27.4 %slice-start.1 = ((s8[8388608]{0:T(1024)(128)(4,1)}), s8[4194304]{0:T(1024)(128)(4,1)S(1)}, s32[]{:S(2)}) async-start(s8[8388608]{0:T(1024)(128)(4,1)} %bitcast.10), calls=%async_computation.1 | async-start | bytes 8388608
  31.5 5.6 %collective-permute-start.13 = (bf16[2,352,128]{2,1,0:T(8,128)(2,1)S(1)}, bf16[2,352,128]{2,1,0:T(8,128)(2,1)S(1)}, u32[]{:S(2)}, u32[]{:S(2)}) collective-permute-start(bf16[2,352,128]{2,1,0:T(8,128)(2,1)S(1)} %pad_maximum_fusion.11), channel_id=1, source_target_pairs={{0,32},{1,97},{32,0},{33,65},{64,96},{65,33},{96,64},{97,1},{2,34}... | collective-permute-start | bytes 540680 | tf_op jit(solution)/shard_map/ppermute | solution.py:31
  34.3 35.9 %collective-permute-start.7 = (bf16[8,704,128]{2,1,0:T(8,128)(2,1)S(1)}, bf16[8,704,128]{2,1,0:T(8,128)(2,1)S(1)}, u32[]{:S(2)}, u32[]{:S(2)}) collective-permute-start(bf16[8,704,128]{2,1,0:T(8,128)(2,1)S(1)} %pad_maximum_fusion.1.refs_0_), channel_id=1, source_target_pairs={{0,96},{1,33},{32,64},{33,1},{64,32},{65,97},{96,0},{97,65},{2,98}... | collective-permute-start | bytes 4325384 | tf_op jit(solution)/shard_map/ppermute | solution.py:31
  34.6 36.7 %collective-permute-start.3 = (bf16[8,704,128]{2,1,0:T(8,128)(2,1)S(1)}, bf16[8,704,128]{2,1,0:T(8,128)(2,1)S(1)}, u32[]{:S(2)}, u32[]{:S(2)}) collective-permute-start(bf16[8,704,128]{2,1,0:T(8,128)(2,1)S(1)} %pad_maximum_fusion.refs_0_), channel_id=1, source_target_pairs={{0,24},{1,9},{8,16},{9,1},{16,8},{17,25},{24,0},{25,17},{2,26},{3,... | collective-permute-start | bytes 4325384 | tf_op jit(solution)/shard_map/ppermute | solution.py:31
  35.3 23.0 %collective-permute-start.10 = (bf16[4,352,128]{2,1,0:T(8,128)(2,1)S(1)}, bf16[4,352,128]{2,1,0:T(8,128)(2,1)S(1)}, u32[]{:S(2)}, u32[]{:S(2)}) collective-permute-start(bf16[4,352,128]{2,1,0:T(8,128)(2,1)S(1)} %pad_maximum_fusion.8), channel_id=1, source_target_pairs={{0,96},{1,33},{32,64},{33,1},{64,32},{65,97},{96,0},{97,65},{2,98}... | collective-permute-start | bytes 1081352 | tf_op jit(solution)/shard_map/ppermute | solution.py:31
  37.2 21.4 %collective-permute-start.14 = (bf16[4,352,128]{2,1,0:T(8,128)(2,1)S(1)}, bf16[4,352,128]{2,1,0:T(8,128)(2,1)S(1)}, u32[]{:S(2)}, u32[]{:S(2)}) collective-permute-start(bf16[4,352,128]{2,1,0:T(8,128)(2,1)S(1)} %pad_maximum_fusion.9), channel_id=1, source_target_pairs={{0,24},{1,9},{8,16},{9,1},{16,8},{17,25},{24,0},{25,17},{2,26},{3,... | collective-permute-start | bytes 1081352 | tf_op jit(solution)/shard_map/ppermute | solution.py:31
  58.4 10.5 %collective-permute-start.11 = (bf16[8,352,128]{2,1,0:T(8,128)(2,1)S(1)}, bf16[8,352,128]{2,1,0:T(8,128)(2,1)S(1)}, u32[]{:S(2)}, u32[]{:S(2)}) collective-permute-start(bf16[8,352,128]{2,1,0:T(8,128)(2,1)S(1)} %pad_maximum_fusion.4.refs_0_), channel_id=1, source_target_pairs={{0,24},{1,9},{8,16},{9,1},{16,8},{17,25},{24,0},{25,17},{2,26},{3,... | collective-permute-start | bytes 2162696 | tf_op jit(solution)/shard_map/ppermute | solution.py:31
  58.6 10.7 %collective-permute-start.15 = (bf16[8,352,128]{2,1,0:T(8,128)(2,1)S(1)}, bf16[8,352,128]{2,1,0:T(8,128)(2,1)S(1)}, u32[]{:S(2)}, u32[]{:S(2)}) collective-permute-start(bf16[8,352,128]{2,1,0:T(8,128)(2,1)S(1)} %pad_maximum_fusion.5.refs_1_), channel_id=1, source_target_pairs={{0,96},{1,33},{32,64},{33,1},{64,32},{65,97},{96,0},{97,65},{2,98}... | collective-permute-start | bytes 2162696 | tf_op jit(solution)/shard_map/ppermute | solution.py:31
  88.9 10.7 %collective-permute-start.22 = (bf16[448,2048]{1,0:T(8,128)(2,1)S(1)}, bf16[448,2048]{1,0:T(8,128)(2,1)S(1)}, u32[]{:S(2)}, u32[]{:S(2)}) collective-permute-start(bf16[448,2048]{1,0:T(8,128)(2,1)S(1)} %shard_map.70), channel_id=1, source_target_pairs={{0,1},{1,0},{2,3},{3,2},{4,5},{5,4},{6,7},{7,6},{8,9},{9,8},{10,11... | collective-permute-start | bytes 5505032 | tf_op jit(solution)/shard_map/ppermute | solution.py:200
  97.1 6.6 %collective-permute-start.19 = (bf16[256,2048]{1,0:T(8,128)(2,1)S(1)}, bf16[256,2048]{1,0:T(8,128)(2,1)S(1)}, u32[]{:S(2)}, u32[]{:S(2)}) collective-permute-start(bf16[256,2048]{1,0:T(8,128)(2,1)S(1)} %shard_map.67), channel_id=1, source_target_pairs={{0,1},{1,0},{2,3},{3,2},{4,5},{5,4},{6,7},{7,6},{8,9},{9,8},{10,11... | collective-permute-start | bytes 3145736 | tf_op jit(solution)/shard_map/ppermute | solution.py:200
  98.0 7.6 %collective-permute-start.25 = (bf16[192,2048]{1,0:T(8,128)(2,1)S(1)}, bf16[192,2048]{1,0:T(8,128)(2,1)S(1)}, u32[]{:S(2)}, u32[]{:S(2)}) collective-permute-start(bf16[192,2048]{1,0:T(8,128)(2,1)S(1)} %shard_map.73), channel_id=1, source_target_pairs={{0,1},{1,0},{2,3},{3,2},{4,5},{5,4},{6,7},{7,6},{8,9},{9,8},{10,11... | collective-permute-start | bytes 2359304 | tf_op jit(solution)/shard_map/ppermute | solution.py:200
  100.4 13.5 %collective-permute-start.23 = (bf16[224,2048]{1,0:T(8,128)(2,1)S(1)}, bf16[224,2048]{1,0:T(8,128)(2,1)S(1)}, u32[]{:S(2)}, u32[]{:S(2)}) collective-permute-start(bf16[224,2048]{1,0:T(8,128)(2,1)S(1)} %shard_map.71), channel_id=1, source_target_pairs={{0,2},{1,7},{2,0},{3,5},{4,6},{5,3},{6,4},{7,1},{8,10},{9,15},{10,... | collective-permute-start | bytes 2752520 | tf_op jit(solution)/shard_map/ppermute | solution.py:31
  103.6 11.7 %collective-permute-start.16 = (bf16[128,2048]{1,0:T(8,128)(2,1)S(1)}, bf16[128,2048]{1,0:T(8,128)(2,1)S(1)}, u32[]{:S(2)}, u32[]{:S(2)}) collective-permute-start(bf16[128,2048]{1,0:T(8,128)(2,1)S(1)} %shard_map.64), channel_id=1, source_target_pairs={{0,1},{1,0},{2,3},{3,2},{4,5},{5,4},{6,7},{7,6},{8,9},{9,8},{10,11... | collective-permute-start | bytes 1572872 | tf_op jit(solution)/shard_map/ppermute | solution.py:200
  104.3 15.8 %collective-permute-start.20 = (bf16[128,2048]{1,0:T(8,128)(2,1)S(1)}, bf16[128,2048]{1,0:T(8,128)(2,1)S(1)}, u32[]{:S(2)}, u32[]{:S(2)}) collective-permute-start(bf16[128,2048]{1,0:T(8,128)(2,1)S(1)} %shard_map.68), channel_id=1, source_target_pairs={{0,2},{1,7},{2,0},{3,5},{4,6},{5,3},{6,4},{7,1},{8,10},{9,15},{10,... | collective-permute-start | bytes 1572872 | tf_op jit(solution)/shard_map/ppermute | solution.py:31
  106.2 22.3 %collective-permute-start.26 = (bf16[96,2048]{1,0:T(8,128)(2,1)S(1)}, bf16[96,2048]{1,0:T(8,128)(2,1)S(1)}, u32[]{:S(2)}, u32[]{:S(2)}) collective-permute-start(bf16[96,2048]{1,0:T(8,128)(2,1)S(1)} %shard_map.74), channel_id=1, source_target_pairs={{0,2},{1,7},{2,0},{3,5},{4,6},{5,3},{6,4},{7,1},{8,10},{9,15},{10,... | collective-permute-start | bytes 1179656 | tf_op jit(solution)/shard_map/ppermute | solution.py:31
  114.9 22.2 %collective-permute-start.24 = (bf16[112,2048]{1,0:T(8,128)(2,1)S(1)}, bf16[112,2048]{1,0:T(8,128)(2,1)S(1)}, u32[]{:S(2)}, u32[]{:S(2)}) collective-permute-start(bf16[112,2048]{1,0:T(8,128)(2,1)S(1)} %get-tuple-element.24), channel_id=1, source_target_pairs={{0,6},{1,3},{2,4},{3,1},{4,2},{5,7},{6,0},{7,5},{8,14},{9,11},{10,... | collective-permute-start | bytes 1376264 | tf_op jit(solution)/shard_map/ppermute | solution.py:31
  115.9 18.2 %collective-permute-start.17 = (bf16[64,2048]{1,0:T(8,128)(2,1)S(1)}, bf16[64,2048]{1,0:T(8,128)(2,1)S(1)}, u32[]{:S(2)}, u32[]{:S(2)}) collective-permute-start(bf16[64,2048]{1,0:T(8,128)(2,1)S(1)} %shard_map.65), channel_id=1, source_target_pairs={{0,2},{1,7},{2,0},{3,5},{4,6},{5,3},{6,4},{7,1},{8,10},{9,15},{10,... | collective-permute-start | bytes 786440 | tf_op jit(solution)/shard_map/ppermute | solution.py:31
  120.7 17.3 %collective-permute-start.21 = (bf16[64,2048]{1,0:T(8,128)(2,1)S(1)}, bf16[64,2048]{1,0:T(8,128)(2,1)S(1)}, u32[]{:S(2)}, u32[]{:S(2)}) collective-permute-start(bf16[64,2048]{1,0:T(8,128)(2,1)S(1)} %get-tuple-element.22), channel_id=1, source_target_pairs={{0,6},{1,3},{2,4},{3,1},{4,2},{5,7},{6,0},{7,5},{8,14},{9,11},{10,... | collective-permute-start | bytes 786440 | tf_op jit(solution)/shard_map/ppermute | solution.py:31
  129.1 7.2 %collective-permute-start.27 = (bf16[48,2048]{1,0:T(8,128)(2,1)S(1)}, bf16[48,2048]{1,0:T(8,128)(2,1)S(1)}, u32[]{:S(2)}, u32[]{:S(2)}) collective-permute-start(bf16[48,2048]{1,0:T(8,128)(2,1)S(1)} %get-tuple-element.26), channel_id=1, source_target_pairs={{0,6},{1,3},{2,4},{3,1},{4,2},{5,7},{6,0},{7,5},{8,14},{9,11},{10,... | collective-permute-start | bytes 589832 | tf_op jit(solution)/shard_map/ppermute | solution.py:31
  134.8 4.0 %collective-permute-start.18 = (bf16[32,2048]{1,0:T(8,128)(2,1)S(1)}, bf16[32,2048]{1,0:T(8,128)(2,1)S(1)}, u32[]{:S(2)}, u32[]{:S(2)}) collective-permute-start(bf16[32,2048]{1,0:T(8,128)(2,1)S(1)} %get-tuple-element.20), channel_id=1, source_target_pairs={{0,6},{1,3},{2,4},{3,1},{4,2},{5,7},{6,0},{7,5},{8,14},{9,11},{10,... | collective-permute-start | bytes 393224 | tf_op jit(solution)/shard_map/ppermute | solution.py:31

commit v3 on v2

--- a/solution.py
+++ b/solution.py
@@ -12,7 +12,7 @@
 LANES = 128
 WIDTH = 704
 ROWS = 256
-CHUNKS = ((0, 48), (48, 112), (160, 64), (224, 32))
+CHUNKS = ((0, 48), (48, 144), (192, 64))
 VMEM = pl.BlockSpec(memory_space=pltpu.VMEM)
 SMEM = pl.BlockSpec(memory_space=pltpu.SMEM)
 ANY = pl.BlockSpec(memory_space=pl.ANY)
@@ -31,13 +31,14 @@
     return lax.ppermute(value, (axis, "c"), pairs)
 
 
-def double(block, route):
-    have = block[None]
-    for n, (axis, step) in enumerate(route):
+def double(have, route, steps=range(4)):
+    for n in steps:
+        axis, step = route[n]
         other = pair_up(have, axis, step)
         if n == 3:
             return have, other
         have = jnp.concatenate([have, other], axis=0)
+    return have
 
 
 def place_of(route, k, pos):
@@ -59,7 +60,7 @@
 ZZYY = (("z", 0), ("z", 1), ("y", 0), ("y", 1))
 YYZZ = (("y", 0), ("y", 1), ("z", 0), ("z", 1))
 ZYZY = (("z", 0), ("y", 0), ("z", 1), ("y", 1))
-YZYZ = (("y", 0), ("z", 0), ("y", 1), ("z", 1))
+ZYYZ = (("z", 0), ("y", 0), ("y", 1), ("z", 1))
 
 
 def scale_kernel(x_ref, out_ref):
@@ -99,31 +100,64 @@
     return lax.dot_general(left, right, (((1,), (1,)), ((), ())), preferred_element_type=jnp.float32)
 
 
-def hidden_kernel(skip, pos, xa_ref, xb_ref, gate_ref, up_ref, scale_ref, out_ref):
+def stack_kernel(g_ref, u_ref, gw_ref, uw_ref):
+    for k in range(8):
+        gw_ref[:, k * LANES:(k + 1) * LANES] = g_ref[k]
+        uw_ref[:, k * LANES:(k + 1) * LANES] = u_ref[k]
+
+
+def stack(gate, up):
+    return call(
+        stack_kernel, [jax.ShapeDtypeStruct((WIDTH, D // 2), jnp.bfloat16)] * 2, 8,
+        in_specs=[VMEM] * 2, out_specs=[VMEM] * 2,
+    )(gate, up)
+
+
+def hidden_kernel(skip, half, pos, xa_ref, xb_ref, gate_ref, up_ref, *refs):
+    gx, ux = refs[-2:]
+    for route, xs in ((ZZYY, gx), (YYZZ, ux)):
+        for k in range(8):
+            at = pl.multiple_of(place_of(route, 8 * half + k, pos) * LANES, LANES)
+            xs[:ROWS, k * LANES:(k + 1) * LANES] = xa_ref[:, pl.ds(at, LANES)]
+            xs[ROWS:, k * LANES:(k + 1) * LANES] = xb_ref[:, pl.ds(at, LANES)]
+    gate = nt(gx[...], gate_ref[...])
+    up = nt(ux[...], up_ref[...])
+    if half == 0:
+        refs[0][...] = gate
+        refs[1][...] = up
+        return
     at = pl.program_id(0) * 2 + skip
-    x = jnp.concatenate([xa_ref[...], xb_ref[...]], axis=0)
     rows = [pl.ds(pl.multiple_of(token_block(at + i, pos) * ROWS, ROWS), ROWS) for i in range(2)]
-    scale = jnp.concatenate([scale_ref[r, :] for r in rows], axis=0)[:, :1]
-    gate = nt(x, gate_ref[...]) * scale
-    up = nt(x, up_ref[...]) * scale
+    scale = jnp.concatenate([refs[2][r, :] for r in rows], axis=0)[:, :1]
+    gate = (gate + refs[0][...]) * scale
+    up = (up + refs[1][...]) * scale
     hidden = (gate / (1.0 + jnp.exp(-gate)) * up).astype(jnp.bfloat16)
-    out_ref[...] = hidden.reshape(out_ref.shape)
-
-
-def hidden_of(pos, skip, count, tokens, gate, up, scale):
-    return call(
-        functools.partial(hidden_kernel, skip), jax.ShapeDtypeStruct((count, ROWS, WIDTH), jnp.bfloat16), 20,
+    refs[3][...] = hidden.reshape(refs[3].shape)
+
+
+def hidden_of(pos, half, skip, count, tokens, weights, more):
+    tile = 2 * ROWS
+    sums = pl.BlockSpec((tile, WIDTH), lambda i, pos: (i + skip // 2, 0))
+    if half:
+        out = jax.ShapeDtypeStruct((count, ROWS, WIDTH), jnp.bfloat16)
+        out_specs = pl.BlockSpec((2, ROWS, WIDTH), lambda i, pos: (i, 0, 0))
+    else:
+        out = [jax.ShapeDtypeStruct((count * ROWS, WIDTH), jnp.float32)] * 2
+        out_specs = [sums] * 2
+    return call(
+        functools.partial(hidden_kernel, skip, half), out, 16,
         grid_spec=pltpu.PrefetchScalarGridSpec(
             num_scalar_prefetch=1,
             grid=(count // 2,),
             in_specs=[
                 pl.BlockSpec((ROWS, D), lambda i, pos: (token_block(2 * i + skip, pos), 0)),
                 pl.BlockSpec((ROWS, D), lambda i, pos: (token_block(2 * i + skip + 1, pos), 0)),
-                VMEM, VMEM, VMEM,
-            ],
-            out_specs=pl.BlockSpec((2, ROWS, WIDTH), lambda i, pos: (i, 0, 0)),
+                VMEM, VMEM,
+            ] + ([sums, sums, VMEM] if half else []),
+            out_specs=out_specs,
+            scratch_shapes=[pltpu.VMEM((tile, D // 2), jnp.bfloat16)] * 2,
         ),
-    )(pos, tokens, tokens, gate, up, scale)
+    )(pos, tokens, tokens, *weights, *more)
 
 
 def down_kernel(rows, picks, at, split, *refs):
@@ -176,31 +210,29 @@
     k = jnp.arange(4, dtype=jnp.int32)
     pos = jnp.where(k == 0, z, jnp.where(k == 1, y, jnp.where(k == 2, x, c)))
     half = WIDTH // 2
-    blocks = [gate_weight.T, up_weight.T, down_weight[:half], down_weight[half:]]
+    blocks = [gate_weight.T, up_weight.T]
     gain = lax.dynamic_slice(norm_gain, ((z * 4 + y) * LANES,), (LANES,))
     for i in range(2):
         blocks[i] = (blocks[i].astype(jnp.float32) * gain).astype(jnp.bfloat16)
     blocks[0], blocks[1], pos = lax.optimization_barrier((blocks[0], blocks[1], pos))
-    gate = double(blocks[0], ZZYY)
-    up = double(blocks[1], YYZZ)
-    down = [double(blocks[2], ZYZY), double(blocks[3], YZYZ)]
-
+    gate = double(blocks[0][None], ZZYY)
+    up = double(blocks[1][None], YYZZ)
+    down = double(down_weight[None], ZYZY, range(2))
+    down = [double(down[:, :half], ZYZY, range(2, 4)), double(down[:, half:], ZYYZ, range(2, 4))]
     scale = scales(tokens)
-    gw = place(pos, [ZZYY], gate[:1], 0, None)
-    gw = place(pos, [ZZYY], gate[1:], 8, gw)
-    uw = place(pos, [YYZZ], up[:1], 0, None)
-    uw = place(pos, [YYZZ], up[1:], 8, uw)
-    hid = [hidden_of(pos, n, m, tokens, gw, uw, scale) for n, m in ((0, 2), (2, 6))]
-    dw = place(pos, [ZYZY, YZYZ], [d[0] for d in down], 0, None)
-    dw = place(pos, [ZYZY, YZYZ], [d[1] for d in down], 8, dw)
+    partial = hidden_of(pos, 0, 0, 8, tokens, stack(gate[0], up[0]), [])
+    rest = stack(gate[1], up[1])
+    hid = [hidden_of(pos, 1, n, 4, tokens, rest, [*partial, scale]) for n in (0, 4)]
+    dw = place(pos, [ZYZY, ZYYZ], [d[0] for d in down], 0, None)
+    dw = place(pos, [ZYZY, ZYYZ], [d[1] for d in down], 8, dw)
 
     out = None
     for chunk in CHUNKS:
-        sent = down_of(chunk, hid, [(0, 0), (0, 1), (1, 0), (1, 1)], dw, [])
+        sent = down_of(chunk, hid[:1], [(0, 0), (0, 1), (0, 2), (0, 3)], dw, [])
         got = lax.ppermute(sent, "c", [(0, 1), (1, 0)])
-        sent = down_of(chunk, hid[1:], [(0, 2), (0, 3)], dw, [(got, 0)])
+        sent = down_of(chunk, hid[1:], [(0, 0), (0, 1)], dw, [(got, 0)])
         got1 = pair_up(sent, "x", 0)
-        sent, own = down_of(chunk, hid[1:], [(0, 4), (0, 5)], dw, [(got, 2), (got1, 0)], True)
+        sent, own = down_of(chunk, hid[1:], [(0, 2), (0, 3)], dw, [(got, 2), (got1, 0)], True)
         got2 = pair_up(sent, "x", 1)
         out = last_of(chunk, own, got2, out)
     return out

time: 142 us -> 136 us (0.958)
  waiting for transfers between devices: 62.4 us -> 59.9 us
  Pallas kernels: 35.1 us -> 33.5 us
    pallas_call x2 -> x5, Pallas kernels: 15 us -> 18.9 us  [the longest x3 17.3 us: hidden_of(): call(functools.partial(hidden_kernel, skip, half), out, 16, grid_spec=plt...]
    pallas_call x6 -> x2, Pallas kernels: 5.75 us -> 1.91 us  [place(): call(functools.partial(place_kernel, first, routes), shape, 8, in_specs=[...]
    ppermute x24 -> x20, starting transfers between devices: 30.7 us -> 27.4 us  [pair_up(): return lax.ppermute(value, (axis, 'c'), pairs)]
    ppermute x4 -> x3, starting transfers between devices: 8.23 us -> 10.3 us  [per_device(): got = lax.ppermute(sent, 'c', [(0, 1), (1, 0)])]
    ppermute x24 -> x20, waiting for transfers between devices: 61.6 us -> 59.7 us  [pair_up(): return lax.ppermute(value, (axis, 'c'), pairs)]
    pallas_call x12 -> x9, Pallas kernels: 9.51 us -> 8.56 us  [down_of(): call(kernel, out, 12, in_specs=[VMEM] * len(ins), out_specs=[VMEM] * 2 if...]
    pallas_call x4 -> x3, Pallas kernels: 3.03 us -> 2.41 us  [last_of(): call(functools.partial(last_kernel, slice(start, start + size)), jax.Shap...]
  transfers between devices with their start and end apart: 28 -> 23, of which waited for: 15 -> 10; matrix products, arithmetic and copies ran while one was open for 1% -> 1% of each run, Pallas kernels for 12% -> 19%
where the time goes in v3:
time: 136 us; the launch traced here: 134 us
  waiting for transfers between devices  59.9 us (44%)
  starting transfers between devices  37.7 us (28%)
  Pallas kernels  33.5 us (25%)
  other arithmetic  1.82 us (1%)
    ppermute x20, waiting for transfers between devices, pair_up(): return lax.ppermute(value, (axis, 'c'), pairs)  59.7 us
    ppermute x20, starting transfers between devices, pair_up(): return lax.ppermute(value, (axis, 'c'), pairs)  27.4 us
    pallas_call x3, Pallas kernels, hidden_of(): call(functools.partial(hidden_kernel, skip, half), out, 16, grid_spec=plt...  17.3 us
    ppermute x3, starting transfers between devices, per_device(): got = lax.ppermute(sent, 'c', [(0, 1), (1, 0)])  10.3 us
    pallas_call x9, Pallas kernels, down_of(): call(kernel, out, 12, in_specs=[VMEM] * len(ins), out_specs=[VMEM] * 2 if...  8.56 us
  transfers between devices with their start and end apart: 23, of which 10 were waited for; matrix products, arithmetic and copies ran while one was open for 1% of the time, Pallas kernels for 19%

profile of v3, /device:TPU:1, one launch (start us, length us, event | category | flops | bytes accessed | tf_op | source)
XLA Modules:
  0.0 134.4 jit_solution(3260787258058993550)
XLA Ops:
  0.0 0.8 dynamic_slice.3
  0.8 1.1 fusion.1
  1.9 4.7 %collective-permute-start = (bf16[1,704,128]{2,1,0:T(8,128)(2,1)S(1)}, bf16[1,704,128]{2,1,0:T(8,128)(2,1)S(1)}, u32[]{:S(2)}, u32[]{:S(2)}) collective-permute-start(bf16[1,704,128]{2,1,0:T(8,128)(2,1)S(1)} %bitcast.13), channel_id=1, source_target_pairs={{0,32},{1,97},{32,0},{33,65},{64,96},{65,33},{96,64},{97,1},{2,34}... | collective-permute-start | bytes 540680 | tf_op jit(solution)/shard_map/ppermute | solution.py:31
  6.6 2.7 %collective-permute-start.4 = (bf16[1,704,128]{2,1,0:T(8,128)(2,1)S(1)}, bf16[1,704,128]{2,1,0:T(8,128)(2,1)S(1)}, u32[]{:S(2)}, u32[]{:S(2)}) collective-permute-start(bf16[1,704,128]{2,1,0:T(8,128)(2,1)S(1)} %bitcast.9), channel_id=1, source_target_pairs={{0,8},{1,25},{8,0},{9,17},{16,24},{17,9},{24,16},{25,1},{2,10},{3,... | collective-permute-start | bytes 540680 | tf_op jit(solution)/shard_map/ppermute | solution.py:31
  9.3 0.1 collective-permute-done
  9.5 0.1 collective-permute-start.1
  9.6 2.6 %collective-permute-done.4 = bf16[1,704,128]{2,1,0:T(8,128)(2,1)S(1)} collective-permute-done((bf16[1,704,128]{2,1,0:T(8,128)(2,1)S(1)}, bf16[1,704,128]{2,1,0:T(8,128)(2,1)S(1)}, u32[]{:S(2)}, u32[]{:S(2)}) %collective-permute-start.4) | collective-permute-done | bytes 180256 | tf_op jit(solution)/shard_map/ppermute | solution.py:31
  12.2 0.1 collective-permute-start.5
  12.3 1.4 %collective-permute-start.8 = (bf16[1,704,128]{2,1,0:T(8,128)(2,1)S(1)}, bf16[1,704,128]{2,1,0:T(8,128)(2,1)S(1)}, u32[]{:S(2)}, u32[]{:S(2)}) collective-permute-start(bf16[1,704,128]{2,1,0:T(8,128)(2,1)S(1)} %bitcast.17), channel_id=1, source_target_pairs={{0,32},{1,97},{32,0},{33,65},{64,96},{65,33},{96,64},{97,1},{2,34}... | collective-permute-start | bytes 540680 | tf_op jit(solution)/shard_map/ppermute | solution.py:31
  13.7 2.5 %collective-permute-done.1 = bf16[2,704,128]{2,1,0:T(8,128)(2,1)S(1)} collective-permute-done((bf16[2,704,128]{2,1,0:T(8,128)(2,1)S(1)}, bf16[2,704,128]{2,1,0:T(8,128)(2,1)S(1)}, u32[]{:S(2)}, u32[]{:S(2)}) %collective-permute-start.1) | collective-permute-done | bytes 360480 | tf_op jit(solution)/shard_map/ppermute | solution.py:31
  16.1 0.1 pad_maximum_fusion.2
  16.2 2.8 %collective-permute-start.2 = (bf16[4,704,128]{2,1,0:T(8,128)(2,1)S(1)}, bf16[4,704,128]{2,1,0:T(8,128)(2,1)S(1)}, u32[]{:S(2)}, u32[]{:S(2)}) collective-permute-start(bf16[4,704,128]{2,1,0:T(8,128)(2,1)S(1)} %pad_maximum_fusion.2), channel_id=1, source_target_pairs={{0,8},{1,25},{8,0},{9,17},{16,24},{17,9},{24,16},{25,1},{2,10},{3,... | collective-permute-start | bytes 2162696 | tf_op jit(solution)/shard_map/ppermute | solution.py:31
  19.0 0.1 pad_maximum_fusion.3
  19.1 4.7 %collective-permute-start.6 = (bf16[4,704,128]{2,1,0:T(8,128)(2,1)S(1)}, bf16[4,704,128]{2,1,0:T(8,128)(2,1)S(1)}, u32[]{:S(2)}, u32[]{:S(2)}) collective-permute-start(bf16[4,704,128]{2,1,0:T(8,128)(2,1)S(1)} %pad_maximum_fusion.3), channel_id=1, source_target_pairs={{0,32},{1,97},{32,0},{33,65},{64,96},{65,33},{96,64},{97,1},{2,34}... | collective-permute-start | bytes 2162696 | tf_op jit(solution)/shard_map/ppermute | solution.py:31
  23.8 0.1 collective-permute-start.9
  23.9 8.8 %collective-permute-done.9 = bf16[2,704,128]{2,1,0:T(8,128)(2,1)S(1)} collective-permute-done((bf16[2,704,128]{2,1,0:T(8,128)(2,1)S(1)}, bf16[2,704,128]{2,1,0:T(8,128)(2,1)S(1)}, u32[]{:S(2)}, u32[]{:S(2)}) %collective-permute-start.9) | collective-permute-done | bytes 360480 | tf_op jit(solution)/shard_map/ppermute | solution.py:31
  32.8 0.1 pad_maximum_fusion.4
  32.9 0.0 slice-start.1
  32.9 0.0 collective-permute-done.2
  32.9 0.1 pad_maximum_fusion.g_ref
  33.0 0.5 collective-permute-start.3
  33.5 0.1 pad_maximum_fusion.1.u_ref
  33.6 0.1 collective-permute-start.7
  33.8 1.5 %collective-permute-start.10 = (bf16[4,352,128]{2,1,0:T(8,128)(2,1)S(1)}, bf16[4,352,128]{2,1,0:T(8,128)(2,1)S(1)}, u32[]{:S(2)}, u32[]{:S(2)}) collective-permute-start(bf16[4,352,128]{2,1,0:T(8,128)(2,1)S(1)} %get-tuple-element.36), channel_id=1, source_target_pairs={{0,96},{1,33},{32,64},{33,1},{64,32},{65,97},{96,0},{97,65},{2,98}... | collective-permute-start | bytes 1081352 | tf_op jit(solution)/shard_map/ppermute | solution.py:31
  35.3 1.1 collective-permute-start.12
  36.4 19.3 %collective-permute-done.10 = bf16[4,352,128]{2,1,0:T(8,128)(2,1)S(1)} collective-permute-done((bf16[4,352,128]{2,1,0:T(8,128)(2,1)S(1)}, bf16[4,352,128]{2,1,0:T(8,128)(2,1)S(1)}, u32[]{:S(2)}, u32[]{:S(2)}) %collective-permute-start.10) | collective-permute-done | bytes 360480 | tf_op jit(solution)/shard_map/ppermute | solution.py:31
  55.7 0.1 pad_maximum_fusion.5.refs_0_
  55.8 1.2 collective-permute-start.11
  57.0 0.1 pad_maximum_fusion.6.refs_1_
  57.0 0.3 collective-permute-start.13
  57.3 1.7 %shard_map.58.refs_2_ = f32[2048,128]{1,0:T(8,128)S(1)} custom-call(bf16[2048,2048]{1,0:T(8,128)(2,1)S(1)} %bitcast.8), custom_call_target="tpu_custom_call" | custom-call | tf_op jit(solution)/shard_map/pallas_call | solution.py:74
  59.1 1.0 shard_map.60.refs_2_
  60.1 0.8 shard_map.56
  60.9 8.1 %shard_map.57 = (f32[2048,704]{1,0:T(8,128)S(1)}, f32[2048,704]{1,0:T(8,128)S(1)}) custom-call(s32[4]{0:T(128)S(1)} %compare_select_fusion.2.pos, bf16[2048,2048]{1,0:T(8,128)(2,1)S(1)} %bitcast.8, bf16[2048,2048]{1,0:T(8,128)(2,1)S(1)} %bitcast.8, bf16[704,1024]{1,0:T(8,128)(2,1)S(1)} %get-tuple-element.25.gate_ref, ...), custom_call_target="tpu_custom_call" | custom-call | tf_op jit(solution)/shard_map/pallas_call | solution.py:147
  69.0 1.0 shard_map.61.refs_1_
  70.0 0.8 shard_map.55
  70.8 4.6 %shard_map.62.refs_0_ = bf16[4,256,704]{2,1,0:T(8,128)(2,1)S(1)} custom-call(s32[4]{0:T(128)S(1)} %compare_select_fusion.2.pos, bf16[2048,2048]{1,0:T(8,128)(2,1)S(1)} %bitcast.8, bf16[2048,2048]{1,0:T(8,128)(2,1)S(1)} %bitcast.8, bf16[704,1024]{1,0:T(8,128)(2,1)S(1)} %get-tuple-element.23.gate_ref, bf16[704,1024]{1,0:T(8,128)(2,1)S(1)} %get-tuple-element.24.up_ref, ...), custom_call_target="tpu_custom_call" | custom-call | tf_op jit(solution)/shard_map/pallas_call | solution.py:147
  75.4 2.0 %shard_map.66 = bf16[576,2048]{1,0:T(8,128)(2,1)S(1)} custom-call(bf16[4,256,704]{2,1,0:T(8,128)(2,1)S(1)} %shard_map.62.refs_0_, bf16[704,2048]{1,0:T(8,128)(2,1)S(1)} %shard_map.61.refs_1_), custom_call_target="tpu_custom_call" | custom-call | tf_op jit(solution)/shard_map/pallas_call | solution.py:186
  77.4 10.2 %collective-permute-start.17 = (bf16[576,2048]{1,0:T(8,128)(2,1)S(1)}, bf16[576,2048]{1,0:T(8,128)(2,1)S(1)}, u32[]{:S(2)}, u32[]{:S(2)}) collective-permute-start(bf16[576,2048]{1,0:T(8,128)(2,1)S(1)} %shard_map.66), channel_id=1, source_target_pairs={{0,1},{1,0},{2,3},{3,2},{4,5},{5,4},{6,7},{7,6},{8,9},{9,8},{10,11... | collective-permute-start | bytes 7077896 | tf_op jit(solution)/shard_map/ppermute | solution.py:232
  87.6 1.0 shard_map.63
  88.6 0.1 collective-permute-start.14
  88.6 4.6 %shard_map.59.refs_0_ = bf16[4,256,704]{2,1,0:T(8,128)(2,1)S(1)} custom-call(s32[4]{0:T(128)S(1)} %compare_select_fusion.2.pos, bf16[2048,2048]{1,0:T(8,128)(2,1)S(1)} %bitcast.8, bf16[2048,2048]{1,0:T(8,128)(2,1)S(1)} %bitcast.8, bf16[704,1024]{1,0:T(8,128)(2,1)S(1)} %get-tuple-element.23.gate_ref, bf16[704,1024]{1,0:T(8,128)(2,1)S(1)} %get-tuple-element.24.up_ref, ...), custom_call_target="tpu_custom_call" | custom-call | tf_op jit(solution)/shard_map/pallas_call | solution.py:147
  93.2 1.1 shard_map.67
  94.3 2.8 %collective-permute-start.18 = (bf16[288,2048]{1,0:T(8,128)(2,1)S(1)}, bf16[288,2048]{1,0:T(8,128)(2,1)S(1)}, u32[]{:S(2)}, u32[]{:S(2)}) collective-permute-start(bf16[288,2048]{1,0:T(8,128)(2,1)S(1)} %shard_map.67), channel_id=1, source_target_pairs={{0,2},{1,7},{2,0},{3,5},{4,6},{5,3},{6,4},{7,1},{8,10},{9,15},{10,... | collective-permute-start | bytes 3538952 | tf_op jit(solution)/shard_map/ppermute | solution.py:31
  97.1 0.8 shard_map.69
  97.9 0.1 collective-permute-start.20
  98.0 0.6 shard_map.64
  98.7 1.4 %collective-permute-start.15 = (bf16[128,2048]{1,0:T(8,128)(2,1)S(1)}, bf16[128,2048]{1,0:T(8,128)(2,1)S(1)}, u32[]{:S(2)}, u32[]{:S(2)}) collective-permute-start(bf16[128,2048]{1,0:T(8,128)(2,1)S(1)} %shard_map.64), channel_id=1, source_target_pairs={{0,2},{1,7},{2,0},{3,5},{4,6},{5,3},{6,4},{7,1},{8,10},{9,15},{10,... | collective-permute-start | bytes 1572872 | tf_op jit(solution)/shard_map/ppermute | solution.py:31
  100.1 0.2 collective-permute-done.20.refs_2_
  100.3 0.6 shard_map.70
  100.9 1.2 collective-permute-start.21
  102.1 8.8 %collective-permute-done.18.refs_3_ = bf16[288,2048]{1,0:T(8,128)(2,1)S(1)} collective-permute-done((bf16[288,2048]{1,0:T(8,128)(2,1)S(1)}, bf16[288,2048]{1,0:T(8,128)(2,1)S(1)}, u32[]{:S(2)}, u32[]{:S(2)}) %collective-permute-start.18) | collective-permute-done | bytes 1179680 | tf_op jit(solution)/shard_map/ppermute | solution.py:31
  110.9 1.2 shard_map.68
  112.1 0.4 collective-permute-start.19
  112.5 4.0 %collective-permute-done.15.refs_3_ = bf16[128,2048]{1,0:T(8,128)(2,1)S(1)} collective-permute-done((bf16[128,2048]{1,0:T(8,128)(2,1)S(1)}, bf16[128,2048]{1,0:T(8,128)(2,1)S(1)}, u32[]{:S(2)}, u32[]{:S(2)}) %collective-permute-start.15) | collective-permute-done | bytes 524320 | tf_op jit(solution)/shard_map/ppermute | solution.py:31
  116.5 0.7 shard_map.65
  117.2 0.4 collective-permute-start.16
  117.6 7.5 %collective-permute-done.21.refs_3_ = bf16[96,2048]{1,0:T(8,128)(2,1)S(1)} collective-permute-done((bf16[96,2048]{1,0:T(8,128)(2,1)S(1)}, bf16[96,2048]{1,0:T(8,128)(2,1)S(1)}, u32[]{:S(2)}, u32[]{:S(2)}) %collective-permute-start.21) | collective-permute-done | bytes 393248 | tf_op jit(solution)/shard_map/ppermute | solution.py:31
  125.1 0.6 shard_map.71
  125.7 0.1 collective-permute-start.22
  125.8 5.9 %collective-permute-done.22.got_ref = bf16[48,2048]{1,0:T(8,128)(2,1)S(1)} collective-permute-done((bf16[48,2048]{1,0:T(8,128)(2,1)S(1)}, bf16[48,2048]{1,0:T(8,128)(2,1)S(1)}, u32[]{:S(2)}, u32[]{:S(2)}) %collective-permute-start.22) | collective-permute-done | bytes 196640 | tf_op jit(solution)/shard_map/ppermute | solution.py:31
  131.7 0.7 shard_map.72.refs_0_
  132.5 0.9 shard_map.73.refs_0_
  133.4 0.8 shard_map.74
  (23 shorter events, 0.2 us)
Async XLA Ops:
  0.0 12.3 %copy-start = (bf16[704,128]{1,0:T(8,128)(2,1)S(1)}, bf16[704,128]{1,0:T(8,128)(2,1)}, u32[]{:S(2)}) copy-start(bf16[704,128]{1,0:T(8,128)(2,1)} %param.9) | copy-start | bytes 540676
  1.9 7.5 %collective-permute-start = (bf16[1,704,128]{2,1,0:T(8,128)(2,1)S(1)}, bf16[1,704,128]{2,1,0:T(8,128)(2,1)S(1)}, u32[]{:S(2)}, u32[]{:S(2)}) collective-permute-start(bf16[1,704,128]{2,1,0:T(8,128)(2,1)S(1)} %bitcast.13), channel_id=1, source_target_pairs={{0,32},{1,97},{32,0},{33,65},{64,96},{65,33},{96,64},{97,1},{2,34}... | collective-permute-start | bytes 540680 | tf_op jit(solution)/shard_map/ppermute | solution.py:31
  6.6 5.6 %collective-permute-start.4 = (bf16[1,704,128]{2,1,0:T(8,128)(2,1)S(1)}, bf16[1,704,128]{2,1,0:T(8,128)(2,1)S(1)}, u32[]{:S(2)}, u32[]{:S(2)}) collective-permute-start(bf16[1,704,128]{2,1,0:T(8,128)(2,1)S(1)} %bitcast.9), channel_id=1, source_target_pairs={{0,8},{1,25},{8,0},{9,17},{16,24},{17,9},{24,16},{25,1},{2,10},{3,... | collective-permute-start | bytes 540680 | tf_op jit(solution)/shard_map/ppermute | solution.py:31
  9.5 6.7 %collective-permute-start.1 = (bf16[2,704,128]{2,1,0:T(8,128)(2,1)S(1)}, bf16[2,704,128]{2,1,0:T(8,128)(2,1)S(1)}, u32[]{:S(2)}, u32[]{:S(2)}) collective-permute-start(bf16[2,704,128]{2,1,0:T(8,128)(2,1)S(1)} %pad_maximum_fusion.7), channel_id=1, source_target_pairs={{0,96},{1,33},{32,64},{33,1},{64,32},{65,97},{96,0},{97,65},{2,98}... | collective-permute-start | bytes 1081352 | tf_op jit(solution)/shard_map/ppermute | solution.py:31
  12.2 6.8 %collective-permute-start.5 = (bf16[2,704,128]{2,1,0:T(8,128)(2,1)S(1)}, bf16[2,704,128]{2,1,0:T(8,128)(2,1)S(1)}, u32[]{:S(2)}, u32[]{:S(2)}) collective-permute-start(bf16[2,704,128]{2,1,0:T(8,128)(2,1)S(1)} %pad_maximum_fusion.8), channel_id=1, source_target_pairs={{0,24},{1,9},{8,16},{9,1},{16,8},{17,25},{24,0},{25,17},{2,26},{3,... | collective-permute-start | bytes 1081352 | tf_op jit(solution)/shard_map/ppermute | solution.py:31
  12.3 11.5 %collective-permute-start.8 = (bf16[1,704,128]{2,1,0:T(8,128)(2,1)S(1)}, bf16[1,704,128]{2,1,0:T(8,128)(2,1)S(1)}, u32[]{:S(2)}, u32[]{:S(2)}) collective-permute-start(bf16[1,704,128]{2,1,0:T(8,128)(2,1)S(1)} %bitcast.17), channel_id=1, source_target_pairs={{0,32},{1,97},{32,0},{33,65},{64,96},{65,33},{96,64},{97,1},{2,34}... | collective-permute-start | bytes 540680 | tf_op jit(solution)/shard_map/ppermute | solution.py:31
  16.1 41.2 %slice-start = ((s8[8388608]{0:T(1024)(128)(4,1)}), s8[4194304]{0:T(1024)(128)(4,1)S(1)}, s32[]{:S(2)}) async-start(s8[8388608]{0:T(1024)(128)(4,1)} %bitcast.7), calls=%async_computation | async-start | bytes 8388608
  16.2 16.7 %collective-permute-start.2 = (bf16[4,704,128]{2,1,0:T(8,128)(2,1)S(1)}, bf16[4,704,128]{2,1,0:T(8,128)(2,1)S(1)}, u32[]{:S(2)}, u32[]{:S(2)}) collective-permute-start(bf16[4,704,128]{2,1,0:T(8,128)(2,1)S(1)} %pad_maximum_fusion.2), channel_id=1, source_target_pairs={{0,8},{1,25},{8,0},{9,17},{16,24},{17,9},{24,16},{25,1},{2,10},{3,... | collective-permute-start | bytes 2162696 | tf_op jit(solution)/shard_map/ppermute | solution.py:31
  19.1 14.4 %collective-permute-start.6 = (bf16[4,704,128]{2,1,0:T(8,128)(2,1)S(1)}, bf16[4,704,128]{2,1,0:T(8,128)(2,1)S(1)}, u32[]{:S(2)}, u32[]{:S(2)}) collective-permute-start(bf16[4,704,128]{2,1,0:T(8,128)(2,1)S(1)} %pad_maximum_fusion.3), channel_id=1, source_target_pairs={{0,32},{1,97},{32,0},{33,65},{64,96},{65,33},{96,64},{97,1},{2,34}... | collective-permute-start | bytes 2162696 | tf_op jit(solution)/shard_map/ppermute | solution.py:31
  23.8 9.0 %collective-permute-start.9 = (bf16[2,704,128]{2,1,0:T(8,128)(2,1)S(1)}, bf16[2,704,128]{2,1,0:T(8,128)(2,1)S(1)}, u32[]{:S(2)}, u32[]{:S(2)}) collective-permute-start(bf16[2,704,128]{2,1,0:T(8,128)(2,1)S(1)} %pad_maximum_fusion.9), channel_id=1, source_target_pairs={{0,8},{1,25},{8,0},{9,17},{16,24},{17,9},{24,16},{25,1},{2,10},{3,... | collective-permute-start | bytes 1081352 | tf_op jit(solution)/shard_map/ppermute | solution.py:31
  32.9 24.5 %slice-start.1 = ((s8[8388608]{0:T(1024)(128)(4,1)}), s8[4194304]{0:T(1024)(128)(4,1)S(1)}, s32[]{:S(2)}) async-start(s8[8388608]{0:T(1024)(128)(4,1)} %bitcast.7), calls=%async_computation.1 | async-start | bytes 8388608
  33.0 37.0 %collective-permute-start.3 = (bf16[8,704,128]{2,1,0:T(8,128)(2,1)S(1)}, bf16[8,704,128]{2,1,0:T(8,128)(2,1)S(1)}, u32[]{:S(2)}, u32[]{:S(2)}) collective-permute-start(bf16[8,704,128]{2,1,0:T(8,128)(2,1)S(1)} %pad_maximum_fusion.g_ref), channel_id=1, source_target_pairs={{0,24},{1,9},{8,16},{9,1},{16,8},{17,25},{24,0},{25,17},{2,26},{3,... | collective-permute-start | bytes 4325384 | tf_op jit(solution)/shard_map/ppermute | solution.py:31
  33.6 36.4 %collective-permute-start.7 = (bf16[8,704,128]{2,1,0:T(8,128)(2,1)S(1)}, bf16[8,704,128]{2,1,0:T(8,128)(2,1)S(1)}, u32[]{:S(2)}, u32[]{:S(2)}) collective-permute-start(bf16[8,704,128]{2,1,0:T(8,128)(2,1)S(1)} %pad_maximum_fusion.1.u_ref), channel_id=1, source_target_pairs={{0,96},{1,33},{32,64},{33,1},{64,32},{65,97},{96,0},{97,65},{2,98}... | collective-permute-start | bytes 4325384 | tf_op jit(solution)/shard_map/ppermute | solution.py:31
  33.8 21.9 %collective-permute-start.10 = (bf16[4,352,128]{2,1,0:T(8,128)(2,1)S(1)}, bf16[4,352,128]{2,1,0:T(8,128)(2,1)S(1)}, u32[]{:S(2)}, u32[]{:S(2)}) collective-permute-start(bf16[4,352,128]{2,1,0:T(8,128)(2,1)S(1)} %get-tuple-element.36), channel_id=1, source_target_pairs={{0,96},{1,33},{32,64},{33,1},{64,32},{65,97},{96,0},{97,65},{2,98}... | collective-permute-start | bytes 1081352 | tf_op jit(solution)/shard_map/ppermute | solution.py:31
  35.3 21.7 %collective-permute-start.12 = (bf16[4,352,128]{2,1,0:T(8,128)(2,1)S(1)}, bf16[4,352,128]{2,1,0:T(8,128)(2,1)S(1)}, u32[]{:S(2)}, u32[]{:S(2)}) collective-permute-start(bf16[4,352,128]{2,1,0:T(8,128)(2,1)S(1)} %get-tuple-element.35), channel_id=1, source_target_pairs={{0,24},{1,9},{8,16},{9,1},{16,8},{17,25},{24,0},{25,17},{2,26},{3,... | collective-permute-start | bytes 1081352 | tf_op jit(solution)/shard_map/ppermute | solution.py:31
  55.8 13.2 %collective-permute-start.11 = (bf16[8,352,128]{2,1,0:T(8,128)(2,1)S(1)}, bf16[8,352,128]{2,1,0:T(8,128)(2,1)S(1)}, u32[]{:S(2)}, u32[]{:S(2)}) collective-permute-start(bf16[8,352,128]{2,1,0:T(8,128)(2,1)S(1)} %pad_maximum_fusion.5.refs_0_), channel_id=1, source_target_pairs={{0,24},{1,9},{8,16},{9,1},{16,8},{17,25},{24,0},{25,17},{2,26},{3,... | collective-permute-start | bytes 2162696 | tf_op jit(solution)/shard_map/ppermute | solution.py:31
  57.0 12.0 %collective-permute-start.13 = (bf16[8,352,128]{2,1,0:T(8,128)(2,1)S(1)}, bf16[8,352,128]{2,1,0:T(8,128)(2,1)S(1)}, u32[]{:S(2)}, u32[]{:S(2)}) collective-permute-start(bf16[8,352,128]{2,1,0:T(8,128)(2,1)S(1)} %pad_maximum_fusion.6.refs_1_), channel_id=1, source_target_pairs={{0,96},{1,33},{32,64},{33,1},{64,32},{65,97},{96,0},{97,65},{2,98}... | collective-permute-start | bytes 2162696 | tf_op jit(solution)/shard_map/ppermute | solution.py:31
  77.4 15.8 %collective-permute-start.17 = (bf16[576,2048]{1,0:T(8,128)(2,1)S(1)}, bf16[576,2048]{1,0:T(8,128)(2,1)S(1)}, u32[]{:S(2)}, u32[]{:S(2)}) collective-permute-start(bf16[576,2048]{1,0:T(8,128)(2,1)S(1)} %shard_map.66), channel_id=1, source_target_pairs={{0,1},{1,0},{2,3},{3,2},{4,5},{5,4},{6,7},{7,6},{8,9},{9,8},{10,11... | collective-permute-start | bytes 7077896 | tf_op jit(solution)/shard_map/ppermute | solution.py:232
  88.6 9.5 %collective-permute-start.14 = (bf16[256,2048]{1,0:T(8,128)(2,1)S(1)}, bf16[256,2048]{1,0:T(8,128)(2,1)S(1)}, u32[]{:S(2)}, u32[]{:S(2)}) collective-permute-start(bf16[256,2048]{1,0:T(8,128)(2,1)S(1)} %shard_map.63), channel_id=1, source_target_pairs={{0,1},{1,0},{2,3},{3,2},{4,5},{5,4},{6,7},{7,6},{8,9},{9,8},{10,11... | collective-permute-start | bytes 3145736 | tf_op jit(solution)/shard_map/ppermute | solution.py:232
  94.3 16.6 %collective-permute-start.18 = (bf16[288,2048]{1,0:T(8,128)(2,1)S(1)}, bf16[288,2048]{1,0:T(8,128)(2,1)S(1)}, u32[]{:S(2)}, u32[]{:S(2)}) collective-permute-start(bf16[288,2048]{1,0:T(8,128)(2,1)S(1)} %shard_map.67), channel_id=1, source_target_pairs={{0,2},{1,7},{2,0},{3,5},{4,6},{5,3},{6,4},{7,1},{8,10},{9,15},{10,... | collective-permute-start | bytes 3538952 | tf_op jit(solution)/shard_map/ppermute | solution.py:31
  97.9 2.4 %collective-permute-start.20 = (bf16[192,2048]{1,0:T(8,128)(2,1)S(1)}, bf16[192,2048]{1,0:T(8,128)(2,1)S(1)}, u32[]{:S(2)}, u32[]{:S(2)}) collective-permute-start(bf16[192,2048]{1,0:T(8,128)(2,1)S(1)} %shard_map.69), channel_id=1, source_target_pairs={{0,1},{1,0},{2,3},{3,2},{4,5},{5,4},{6,7},{7,6},{8,9},{9,8},{10,11... | collective-permute-start | bytes 2359304 | tf_op jit(solution)/shard_map/ppermute | solution.py:232
  98.7 17.9 %collective-permute-start.15 = (bf16[128,2048]{1,0:T(8,128)(2,1)S(1)}, bf16[128,2048]{1,0:T(8,128)(2,1)S(1)}, u32[]{:S(2)}, u32[]{:S(2)}) collective-permute-start(bf16[128,2048]{1,0:T(8,128)(2,1)S(1)} %shard_map.64), channel_id=1, source_target_pairs={{0,2},{1,7},{2,0},{3,5},{4,6},{5,3},{6,4},{7,1},{8,10},{9,15},{10,... | collective-permute-start | bytes 1572872 | tf_op jit(solution)/shard_map/ppermute | solution.py:31
  100.9 24.2 %collective-permute-start.21 = (bf16[96,2048]{1,0:T(8,128)(2,1)S(1)}, bf16[96,2048]{1,0:T(8,128)(2,1)S(1)}, u32[]{:S(2)}, u32[]{:S(2)}) collective-permute-start(bf16[96,2048]{1,0:T(8,128)(2,1)S(1)} %shard_map.70), channel_id=1, source_target_pairs={{0,2},{1,7},{2,0},{3,5},{4,6},{5,3},{6,4},{7,1},{8,10},{9,15},{10,... | collective-permute-start | bytes 1179656 | tf_op jit(solution)/shard_map/ppermute | solution.py:31
  112.1 20.4 %collective-permute-start.19 = (bf16[144,2048]{1,0:T(8,128)(2,1)S(1)}, bf16[144,2048]{1,0:T(8,128)(2,1)S(1)}, u32[]{:S(2)}, u32[]{:S(2)}) collective-permute-start(bf16[144,2048]{1,0:T(8,128)(2,1)S(1)} %get-tuple-element.32), channel_id=1, source_target_pairs={{0,6},{1,3},{2,4},{3,1},{4,2},{5,7},{6,0},{7,5},{8,14},{9,11},{10,... | collective-permute-start | bytes 1769480 | tf_op jit(solution)/shard_map/ppermute | solution.py:31
  117.2 16.2 %collective-permute-start.16 = (bf16[64,2048]{1,0:T(8,128)(2,1)S(1)}, bf16[64,2048]{1,0:T(8,128)(2,1)S(1)}, u32[]{:S(2)}, u32[]{:S(2)}) collective-permute-start(bf16[64,2048]{1,0:T(8,128)(2,1)S(1)} %get-tuple-element.30), channel_id=1, source_target_pairs={{0,6},{1,3},{2,4},{3,1},{4,2},{5,7},{6,0},{7,5},{8,14},{9,11},{10,... | collective-permute-start | bytes 786440 | tf_op jit(solution)/shard_map/ppermute | solution.py:31
  125.7 6.0 %collective-permute-start.22 = (bf16[48,2048]{1,0:T(8,128)(2,1)S(1)}, bf16[48,2048]{1,0:T(8,128)(2,1)S(1)}, u32[]{:S(2)}, u32[]{:S(2)}) collective-permute-start(bf16[48,2048]{1,0:T(8,128)(2,1)S(1)} %get-tuple-element.34), channel_id=1, source_target_pairs={{0,6},{1,3},{2,4},{3,1},{4,2},{5,7},{6,0},{7,5},{8,14},{9,11},{10,... | collective-permute-start | bytes 589832 | tf_op jit(solution)/shard_map/ppermute | solution.py:31

commit v4 on v3

--- a/solution.py
+++ b/solution.py
@@ -12,7 +12,7 @@
 LANES = 128
 WIDTH = 704
 ROWS = 256
-CHUNKS = ((0, 48), (48, 144), (192, 64))
+CHUNKS = ((0, 64), (64, 144), (208, 48))
 VMEM = pl.BlockSpec(memory_space=pltpu.VMEM)
 SMEM = pl.BlockSpec(memory_space=pltpu.SMEM)
 ANY = pl.BlockSpec(memory_space=pl.ANY)
@@ -222,7 +222,7 @@
     scale = scales(tokens)
     partial = hidden_of(pos, 0, 0, 8, tokens, stack(gate[0], up[0]), [])
     rest = stack(gate[1], up[1])
-    hid = [hidden_of(pos, 1, n, 4, tokens, rest, [*partial, scale]) for n in (0, 4)]
+    hid = [hidden_of(pos, 1, n, m, tokens, rest, [*partial, scale]) for n, m in ((0, 4), (4, 2), (6, 2))]
     dw = place(pos, [ZYZY, ZYYZ], [d[0] for d in down], 0, None)
     dw = place(pos, [ZYZY, ZYYZ], [d[1] for d in down], 8, dw)
 
@@ -230,9 +230,9 @@
     for chunk in CHUNKS:
         sent = down_of(chunk, hid[:1], [(0, 0), (0, 1), (0, 2), (0, 3)], dw, [])
         got = lax.ppermute(sent, "c", [(0, 1), (1, 0)])
-        sent = down_of(chunk, hid[1:], [(0, 0), (0, 1)], dw, [(got, 0)])
+        sent = down_of(chunk, hid[1:2], [(0, 0), (0, 1)], dw, [(got, 0)])
         got1 = pair_up(sent, "x", 0)
-        sent, own = down_of(chunk, hid[1:], [(0, 2), (0, 3)], dw, [(got, 2), (got1, 0)], True)
+        sent, own = down_of(chunk, hid[2:], [(0, 0), (0, 1)], dw, [(got, 2), (got1, 0)], True)
         got2 = pair_up(sent, "x", 1)
         out = last_of(chunk, own, got2, out)
     return out

time: 136 us -> 133 us (0.978)
  waiting for transfers between devices: 59.9 us -> 55.9 us
    ppermute x20, waiting for transfers between devices: 59.7 us -> 55.4 us  [pair_up(): return lax.ppermute(value, (axis, 'c'), pairs)]
    pallas_call x3 -> x4, Pallas kernels: 17.3 us -> 17.8 us  [hidden_of(): call(functools.partial(hidden_kernel, skip, half), out, 16, grid_spec=plt...]
  transfers between devices with their start and end apart: 23 -> 23, of which waited for: 10 -> 11; matrix products, arithmetic and copies ran while one was open for 1% -> 1% of each run, Pallas kernels for 19% -> 20%
where the time goes in v4:
time: 133 us; the launch traced here: 131 us
  waiting for transfers between devices  55.9 us (42%)
  starting transfers between devices  38 us (29%)
  Pallas kernels  33.9 us (25%)
  other arithmetic  1.82 us (1%)
    ppermute x20, waiting for transfers between devices, pair_up(): return lax.ppermute(value, (axis, 'c'), pairs)  55.4 us
    ppermute x20, starting transfers between devices, pair_up(): return lax.ppermute(value, (axis, 'c'), pairs)  27.6 us
    pallas_call x4, Pallas kernels, hidden_of(): call(functools.partial(hidden_kernel, skip, half), out, 16, grid_spec=plt...  17.8 us
    ppermute x3, starting transfers between devices, per_device(): got = lax.ppermute(sent, 'c', [(0, 1), (1, 0)])  10.3 us
    pallas_call x9, Pallas kernels, down_of(): call(kernel, out, 12, in_specs=[VMEM] * len(ins), out_specs=[VMEM] * 2 if...  8.41 us
  transfers between devices with their start and end apart: 23, of which 11 were waited for; matrix products, arithmetic and copies ran while one was open for 1% of the time, Pallas kernels for 20%

profile of v4, /device:TPU:1, one launch (start us, length us, event | category | flops | bytes accessed | tf_op | source)
XLA Modules:
  0.0 131.0 jit_solution(18120879823402629978)
XLA Ops:
  0.0 0.8 dynamic_slice.3
  0.8 1.1 fusion.1
  1.9 4.7 %collective-permute-start = (bf16[1,704,128]{2,1,0:T(8,128)(2,1)S(1)}, bf16[1,704,128]{2,1,0:T(8,128)(2,1)S(1)}, u32[]{:S(2)}, u32[]{:S(2)}) collective-permute-start(bf16[1,704,128]{2,1,0:T(8,128)(2,1)S(1)} %bitcast.13), channel_id=1, source_target_pairs={{0,32},{1,97},{32,0},{33,65},{64,96},{65,33},{96,64},{97,1},{2,34}... | collective-permute-start | bytes 540680 | tf_op jit(solution)/shard_map/ppermute | solution.py:31
  6.6 2.7 %collective-permute-start.4 = (bf16[1,704,128]{2,1,0:T(8,128)(2,1)S(1)}, bf16[1,704,128]{2,1,0:T(8,128)(2,1)S(1)}, u32[]{:S(2)}, u32[]{:S(2)}) collective-permute-start(bf16[1,704,128]{2,1,0:T(8,128)(2,1)S(1)} %bitcast.9), channel_id=1, source_target_pairs={{0,8},{1,25},{8,0},{9,17},{16,24},{17,9},{24,16},{25,1},{2,10},{3,... | collective-permute-start | bytes 540680 | tf_op jit(solution)/shard_map/ppermute | solution.py:31
  9.3 0.1 collective-permute-done
  9.5 0.1 collective-permute-start.1
  9.6 2.6 %collective-permute-done.4 = bf16[1,704,128]{2,1,0:T(8,128)(2,1)S(1)} collective-permute-done((bf16[1,704,128]{2,1,0:T(8,128)(2,1)S(1)}, bf16[1,704,128]{2,1,0:T(8,128)(2,1)S(1)}, u32[]{:S(2)}, u32[]{:S(2)}) %collective-permute-start.4) | collective-permute-done | bytes 180256 | tf_op jit(solution)/shard_map/ppermute | solution.py:31
  12.2 0.1 collective-permute-start.5
  12.3 1.4 %collective-permute-start.8 = (bf16[1,704,128]{2,1,0:T(8,128)(2,1)S(1)}, bf16[1,704,128]{2,1,0:T(8,128)(2,1)S(1)}, u32[]{:S(2)}, u32[]{:S(2)}) collective-permute-start(bf16[1,704,128]{2,1,0:T(8,128)(2,1)S(1)} %bitcast.17), channel_id=1, source_target_pairs={{0,32},{1,97},{32,0},{33,65},{64,96},{65,33},{96,64},{97,1},{2,34}... | collective-permute-start | bytes 540680 | tf_op jit(solution)/shard_map/ppermute | solution.py:31
  13.7 2.5 %collective-permute-done.1 = bf16[2,704,128]{2,1,0:T(8,128)(2,1)S(1)} collective-permute-done((bf16[2,704,128]{2,1,0:T(8,128)(2,1)S(1)}, bf16[2,704,128]{2,1,0:T(8,128)(2,1)S(1)}, u32[]{:S(2)}, u32[]{:S(2)}) %collective-permute-start.1) | collective-permute-done | bytes 360480 | tf_op jit(solution)/shard_map/ppermute | solution.py:31
  16.1 0.1 pad_maximum_fusion.2
  16.2 2.8 %collective-permute-start.2 = (bf16[4,704,128]{2,1,0:T(8,128)(2,1)S(1)}, bf16[4,704,128]{2,1,0:T(8,128)(2,1)S(1)}, u32[]{:S(2)}, u32[]{:S(2)}) collective-permute-start(bf16[4,704,128]{2,1,0:T(8,128)(2,1)S(1)} %pad_maximum_fusion.2), channel_id=1, source_target_pairs={{0,8},{1,25},{8,0},{9,17},{16,24},{17,9},{24,16},{25,1},{2,10},{3,... | collective-permute-start | bytes 2162696 | tf_op jit(solution)/shard_map/ppermute | solution.py:31
  19.0 0.1 pad_maximum_fusion.3
  19.1 4.7 %collective-permute-start.6 = (bf16[4,704,128]{2,1,0:T(8,128)(2,1)S(1)}, bf16[4,704,128]{2,1,0:T(8,128)(2,1)S(1)}, u32[]{:S(2)}, u32[]{:S(2)}) collective-permute-start(bf16[4,704,128]{2,1,0:T(8,128)(2,1)S(1)} %pad_maximum_fusion.3), channel_id=1, source_target_pairs={{0,32},{1,97},{32,0},{33,65},{64,96},{65,33},{96,64},{97,1},{2,34}... | collective-permute-start | bytes 2162696 | tf_op jit(solution)/shard_map/ppermute | solution.py:31
  23.8 0.1 collective-permute-start.9
  23.9 8.8 %collective-permute-done.9 = bf16[2,704,128]{2,1,0:T(8,128)(2,1)S(1)} collective-permute-done((bf16[2,704,128]{2,1,0:T(8,128)(2,1)S(1)}, bf16[2,704,128]{2,1,0:T(8,128)(2,1)S(1)}, u32[]{:S(2)}, u32[]{:S(2)}) %collective-permute-start.9) | collective-permute-done | bytes 360480 | tf_op jit(solution)/shard_map/ppermute | solution.py:31
  32.8 0.1 pad_maximum_fusion.4
  32.9 0.1 pad_maximum_fusion.g_ref
  33.0 0.5 collective-permute-start.3
  33.5 0.1 pad_maximum_fusion.1.u_ref
  33.6 0.1 collective-permute-start.7
  33.8 1.5 %collective-permute-start.10 = (bf16[4,352,128]{2,1,0:T(8,128)(2,1)S(1)}, bf16[4,352,128]{2,1,0:T(8,128)(2,1)S(1)}, u32[]{:S(2)}, u32[]{:S(2)}) collective-permute-start(bf16[4,352,128]{2,1,0:T(8,128)(2,1)S(1)} %get-tuple-element.36), channel_id=1, source_target_pairs={{0,96},{1,33},{32,64},{33,1},{64,32},{65,97},{96,0},{97,65},{2,98}... | collective-permute-start | bytes 1081352 | tf_op jit(solution)/shard_map/ppermute | solution.py:31
  35.3 1.1 collective-permute-start.12
  36.4 19.3 %collective-permute-done.10 = bf16[4,352,128]{2,1,0:T(8,128)(2,1)S(1)} collective-permute-done((bf16[4,352,128]{2,1,0:T(8,128)(2,1)S(1)}, bf16[4,352,128]{2,1,0:T(8,128)(2,1)S(1)}, u32[]{:S(2)}, u32[]{:S(2)}) %collective-permute-start.10) | collective-permute-done | bytes 360480 | tf_op jit(solution)/shard_map/ppermute | solution.py:31
  55.7 0.1 pad_maximum_fusion.5.refs_0_
  55.8 1.2 collective-permute-start.11
  57.0 0.1 pad_maximum_fusion.6.refs_1_
  57.0 0.3 collective-permute-start.13
  57.3 1.7 %shard_map.58.refs_2_ = f32[2048,128]{1,0:T(8,128)S(1)} custom-call(bf16[2048,2048]{1,0:T(8,128)(2,1)S(1)} %bitcast.8), custom_call_target="tpu_custom_call" | custom-call | tf_op jit(solution)/shard_map/pallas_call | solution.py:74
  59.1 1.0 shard_map.60.refs_2_
  60.1 0.8 shard_map.56
  60.9 8.1 %shard_map.57 = (f32[2048,704]{1,0:T(8,128)S(1)}, f32[2048,704]{1,0:T(8,128)S(1)}) custom-call(s32[4]{0:T(128)S(1)} %compare_select_fusion.2.pos, bf16[2048,2048]{1,0:T(8,128)(2,1)S(1)} %bitcast.8, bf16[2048,2048]{1,0:T(8,128)(2,1)S(1)} %bitcast.8, bf16[704,1024]{1,0:T(8,128)(2,1)S(1)} %get-tuple-element.25.gate_ref, ...), custom_call_target="tpu_custom_call" | custom-call | tf_op jit(solution)/shard_map/pallas_call | solution.py:147
  69.0 1.0 shard_map.61.refs_1_
  70.0 0.8 shard_map.55
  70.8 4.6 %shard_map.62.refs_0_ = bf16[4,256,704]{2,1,0:T(8,128)(2,1)S(1)} custom-call(s32[4]{0:T(128)S(1)} %compare_select_fusion.2.pos, bf16[2048,2048]{1,0:T(8,128)(2,1)S(1)} %bitcast.8, bf16[2048,2048]{1,0:T(8,128)(2,1)S(1)} %bitcast.8, bf16[704,1024]{1,0:T(8,128)(2,1)S(1)} %get-tuple-element.23.gate_ref, bf16[704,1024]{1,0:T(8,128)(2,1)S(1)} %get-tuple-element.24.up_ref, ...), custom_call_target="tpu_custom_call" | custom-call | tf_op jit(solution)/shard_map/pallas_call | solution.py:147
  75.4 2.0 %shard_map.67 = bf16[576,2048]{1,0:T(8,128)(2,1)S(1)} custom-call(bf16[4,256,704]{2,1,0:T(8,128)(2,1)S(1)} %shard_map.62.refs_0_, bf16[704,2048]{1,0:T(8,128)(2,1)S(1)} %shard_map.61.refs_1_), custom_call_target="tpu_custom_call" | custom-call | tf_op jit(solution)/shard_map/pallas_call | solution.py:186
  77.4 10.1 %collective-permute-start.17 = (bf16[576,2048]{1,0:T(8,128)(2,1)S(1)}, bf16[576,2048]{1,0:T(8,128)(2,1)S(1)}, u32[]{:S(2)}, u32[]{:S(2)}) collective-permute-start(bf16[576,2048]{1,0:T(8,128)(2,1)S(1)} %shard_map.67), channel_id=1, source_target_pairs={{0,1},{1,0},{2,3},{3,2},{4,5},{5,4},{6,7},{7,6},{8,9},{9,8},{10,11... | collective-permute-start | bytes 7077896 | tf_op jit(solution)/shard_map/ppermute | solution.py:232
  87.6 1.0 shard_map.70
  88.5 0.1 collective-permute-start.20
  88.6 2.5 %shard_map.64.refs_0_ = bf16[2,256,704]{2,1,0:T(8,128)(2,1)S(1)} custom-call(s32[4]{0:T(128)S(1)} %compare_select_fusion.2.pos, bf16[2048,2048]{1,0:T(8,128)(2,1)S(1)} %bitcast.8, bf16[2048,2048]{1,0:T(8,128)(2,1)S(1)} %bitcast.8, bf16[704,1024]{1,0:T(8,128)(2,1)S(1)} %get-tuple-element.23.gate_ref, bf16[704,1024]{1,0:T(8,128)(2,1)S(1)} %get-tuple-element.24.up_ref, ...), custom_call_target="tpu_custom_call" | custom-call | tf_op jit(solution)/shard_map/pallas_call | solution.py:147
  91.2 0.5 collective-permute-done.17.refs_2_
  91.7 1.1 shard_map.68
  92.8 2.8 %collective-permute-start.18 = (bf16[288,2048]{1,0:T(8,128)(2,1)S(1)}, bf16[288,2048]{1,0:T(8,128)(2,1)S(1)}, u32[]{:S(2)}, u32[]{:S(2)}) collective-permute-start(bf16[288,2048]{1,0:T(8,128)(2,1)S(1)} %shard_map.68), channel_id=1, source_target_pairs={{0,2},{1,7},{2,0},{3,5},{4,6},{5,3},{6,4},{7,1},{8,10},{9,15},{10,... | collective-permute-start | bytes 3538952 | tf_op jit(solution)/shard_map/ppermute | solution.py:31
  95.6 0.8 shard_map.63
  96.4 0.1 collective-permute-start.14
  96.5 0.6 shard_map.71
  97.1 1.3 collective-permute-start.21
  98.4 2.5 %shard_map.59.refs_0_ = bf16[2,256,704]{2,1,0:T(8,128)(2,1)S(1)} custom-call(s32[4]{0:T(128)S(1)} %compare_select_fusion.2.pos, bf16[2048,2048]{1,0:T(8,128)(2,1)S(1)} %bitcast.8, bf16[2048,2048]{1,0:T(8,128)(2,1)S(1)} %bitcast.8, bf16[704,1024]{1,0:T(8,128)(2,1)S(1)} %get-tuple-element.23.gate_ref, bf16[704,1024]{1,0:T(8,128)(2,1)S(1)} %get-tuple-element.24.up_ref, ...), custom_call_target="tpu_custom_call" | custom-call | tf_op jit(solution)/shard_map/pallas_call | solution.py:147
  100.9 0.6 shard_map.65
  101.5 1.6 %collective-permute-start.15 = (bf16[96,2048]{1,0:T(8,128)(2,1)S(1)}, bf16[96,2048]{1,0:T(8,128)(2,1)S(1)}, u32[]{:S(2)}, u32[]{:S(2)}) collective-permute-start(bf16[96,2048]{1,0:T(8,128)(2,1)S(1)} %shard_map.65), channel_id=1, source_target_pairs={{0,2},{1,7},{2,0},{3,5},{4,6},{5,3},{6,4},{7,1},{8,10},{9,15},{10,... | collective-permute-start | bytes 1179656 | tf_op jit(solution)/shard_map/ppermute | solution.py:31
  103.1 6.3 %collective-permute-done.18.refs_3_ = bf16[288,2048]{1,0:T(8,128)(2,1)S(1)} collective-permute-done((bf16[288,2048]{1,0:T(8,128)(2,1)S(1)}, bf16[288,2048]{1,0:T(8,128)(2,1)S(1)}, u32[]{:S(2)}, u32[]{:S(2)}) %collective-permute-start.18) | collective-permute-done | bytes 1179680 | tf_op jit(solution)/shard_map/ppermute | solution.py:31
  109.4 1.1 shard_map.69
  110.5 0.4 collective-permute-start.19
  110.9 4.1 %collective-permute-done.21.refs_3_ = bf16[128,2048]{1,0:T(8,128)(2,1)S(1)} collective-permute-done((bf16[128,2048]{1,0:T(8,128)(2,1)S(1)}, bf16[128,2048]{1,0:T(8,128)(2,1)S(1)}, u32[]{:S(2)}, u32[]{:S(2)}) %collective-permute-start.21) | collective-permute-done | bytes 524320 | tf_op jit(solution)/shard_map/ppermute | solution.py:31
  115.0 0.6 shard_map.72
  115.6 0.4 collective-permute-start.22
  116.0 7.7 %collective-permute-done.15.refs_3_ = bf16[96,2048]{1,0:T(8,128)(2,1)S(1)} collective-permute-done((bf16[96,2048]{1,0:T(8,128)(2,1)S(1)}, bf16[96,2048]{1,0:T(8,128)(2,1)S(1)}, u32[]{:S(2)}, u32[]{:S(2)}) %collective-permute-start.15) | collective-permute-done | bytes 393248 | tf_op jit(solution)/shard_map/ppermute | solution.py:31
  123.7 0.6 shard_map.66
  124.3 0.1 collective-permute-start.16
  124.4 3.8 %collective-permute-done.22.got_ref = bf16[64,2048]{1,0:T(8,128)(2,1)S(1)} collective-permute-done((bf16[64,2048]{1,0:T(8,128)(2,1)S(1)}, bf16[64,2048]{1,0:T(8,128)(2,1)S(1)}, u32[]{:S(2)}, u32[]{:S(2)}) %collective-permute-start.22) | collective-permute-done | bytes 262176 | tf_op jit(solution)/shard_map/ppermute | solution.py:31
  128.3 0.8 shard_map.73.refs_0_
  129.0 0.9 shard_map.74.refs_0_
  130.0 0.1 collective-permute-done.16.got_ref
  130.1 0.7 shard_map.75
  (24 shorter events, 0.2 us)
Async XLA Ops:
  0.0 12.3 %copy-start = (bf16[704,128]{1,0:T(8,128)(2,1)S(1)}, bf16[704,128]{1,0:T(8,128)(2,1)}, u32[]{:S(2)}) copy-start(bf16[704,128]{1,0:T(8,128)(2,1)} %param.9) | copy-start | bytes 540676
  1.9 7.5 %collective-permute-start = (bf16[1,704,128]{2,1,0:T(8,128)(2,1)S(1)}, bf16[1,704,128]{2,1,0:T(8,128)(2,1)S(1)}, u32[]{:S(2)}, u32[]{:S(2)}) collective-permute-start(bf16[1,704,128]{2,1,0:T(8,128)(2,1)S(1)} %bitcast.13), channel_id=1, source_target_pairs={{0,32},{1,97},{32,0},{33,65},{64,96},{65,33},{96,64},{97,1},{2,34}... | collective-permute-start | bytes 540680 | tf_op jit(solution)/shard_map/ppermute | solution.py:31
  6.6 5.6 %collective-permute-start.4 = (bf16[1,704,128]{2,1,0:T(8,128)(2,1)S(1)}, bf16[1,704,128]{2,1,0:T(8,128)(2,1)S(1)}, u32[]{:S(2)}, u32[]{:S(2)}) collective-permute-start(bf16[1,704,128]{2,1,0:T(8,128)(2,1)S(1)} %bitcast.9), channel_id=1, source_target_pairs={{0,8},{1,25},{8,0},{9,17},{16,24},{17,9},{24,16},{25,1},{2,10},{3,... | collective-permute-start | bytes 540680 | tf_op jit(solution)/shard_map/ppermute | solution.py:31
  9.5 6.7 %collective-permute-start.1 = (bf16[2,704,128]{2,1,0:T(8,128)(2,1)S(1)}, bf16[2,704,128]{2,1,0:T(8,128)(2,1)S(1)}, u32[]{:S(2)}, u32[]{:S(2)}) collective-permute-start(bf16[2,704,128]{2,1,0:T(8,128)(2,1)S(1)} %pad_maximum_fusion.7), channel_id=1, source_target_pairs={{0,96},{1,33},{32,64},{33,1},{64,32},{65,97},{96,0},{97,65},{2,98}... | collective-permute-start | bytes 1081352 | tf_op jit(solution)/shard_map/ppermute | solution.py:31
  12.2 6.8 %collective-permute-start.5 = (bf16[2,704,128]{2,1,0:T(8,128)(2,1)S(1)}, bf16[2,704,128]{2,1,0:T(8,128)(2,1)S(1)}, u32[]{:S(2)}, u32[]{:S(2)}) collective-permute-start(bf16[2,704,128]{2,1,0:T(8,128)(2,1)S(1)} %pad_maximum_fusion.8), channel_id=1, source_target_pairs={{0,24},{1,9},{8,16},{9,1},{16,8},{17,25},{24,0},{25,17},{2,26},{3,... | collective-permute-start | bytes 1081352 | tf_op jit(solution)/shard_map/ppermute | solution.py:31
  12.3 11.5 %collective-permute-start.8 = (bf16[1,704,128]{2,1,0:T(8,128)(2,1)S(1)}, bf16[1,704,128]{2,1,0:T(8,128)(2,1)S(1)}, u32[]{:S(2)}, u32[]{:S(2)}) collective-permute-start(bf16[1,704,128]{2,1,0:T(8,128)(2,1)S(1)} %bitcast.17), channel_id=1, source_target_pairs={{0,32},{1,97},{32,0},{33,65},{64,96},{65,33},{96,64},{97,1},{2,34}... | collective-permute-start | bytes 540680 | tf_op jit(solution)/shard_map/ppermute | solution.py:31
  16.1 41.2 %slice-start = ((s8[8388608]{0:T(1024)(128)(4,1)}), s8[4194304]{0:T(1024)(128)(4,1)S(1)}, s32[]{:S(2)}) async-start(s8[8388608]{0:T(1024)(128)(4,1)} %bitcast.7), calls=%async_computation | async-start | bytes 8388608
  16.2 16.7 %collective-permute-start.2 = (bf16[4,704,128]{2,1,0:T(8,128)(2,1)S(1)}, bf16[4,704,128]{2,1,0:T(8,128)(2,1)S(1)}, u32[]{:S(2)}, u32[]{:S(2)}) collective-permute-start(bf16[4,704,128]{2,1,0:T(8,128)(2,1)S(1)} %pad_maximum_fusion.2), channel_id=1, source_target_pairs={{0,8},{1,25},{8,0},{9,17},{16,24},{17,9},{24,16},{25,1},{2,10},{3,... | collective-permute-start | bytes 2162696 | tf_op jit(solution)/shard_map/ppermute | solution.py:31
  19.1 14.4 %collective-permute-start.6 = (bf16[4,704,128]{2,1,0:T(8,128)(2,1)S(1)}, bf16[4,704,128]{2,1,0:T(8,128)(2,1)S(1)}, u32[]{:S(2)}, u32[]{:S(2)}) collective-permute-start(bf16[4,704,128]{2,1,0:T(8,128)(2,1)S(1)} %pad_maximum_fusion.3), channel_id=1, source_target_pairs={{0,32},{1,97},{32,0},{33,65},{64,96},{65,33},{96,64},{97,1},{2,34}... | collective-permute-start | bytes 2162696 | tf_op jit(solution)/shard_map/ppermute | solution.py:31
  23.8 9.0 %collective-permute-start.9 = (bf16[2,704,128]{2,1,0:T(8,128)(2,1)S(1)}, bf16[2,704,128]{2,1,0:T(8,128)(2,1)S(1)}, u32[]{:S(2)}, u32[]{:S(2)}) collective-permute-start(bf16[2,704,128]{2,1,0:T(8,128)(2,1)S(1)} %pad_maximum_fusion.9), channel_id=1, source_target_pairs={{0,8},{1,25},{8,0},{9,17},{16,24},{17,9},{24,16},{25,1},{2,10},{3,... | collective-permute-start | bytes 1081352 | tf_op jit(solution)/shard_map/ppermute | solution.py:31
  32.9 24.5 %slice-start.1 = ((s8[8388608]{0:T(1024)(128)(4,1)}), s8[4194304]{0:T(1024)(128)(4,1)S(1)}, s32[]{:S(2)}) async-start(s8[8388608]{0:T(1024)(128)(4,1)} %bitcast.7), calls=%async_computation.1 | async-start | bytes 8388608
  33.0 37.0 %collective-permute-start.3 = (bf16[8,704,128]{2,1,0:T(8,128)(2,1)S(1)}, bf16[8,704,128]{2,1,0:T(8,128)(2,1)S(1)}, u32[]{:S(2)}, u32[]{:S(2)}) collective-permute-start(bf16[8,704,128]{2,1,0:T(8,128)(2,1)S(1)} %pad_maximum_fusion.g_ref), channel_id=1, source_target_pairs={{0,24},{1,9},{8,16},{9,1},{16,8},{17,25},{24,0},{25,17},{2,26},{3,... | collective-permute-start | bytes 4325384 | tf_op jit(solution)/shard_map/ppermute | solution.py:31
  33.6 36.4 %collective-permute-start.7 = (bf16[8,704,128]{2,1,0:T(8,128)(2,1)S(1)}, bf16[8,704,128]{2,1,0:T(8,128)(2,1)S(1)}, u32[]{:S(2)}, u32[]{:S(2)}) collective-permute-start(bf16[8,704,128]{2,1,0:T(8,128)(2,1)S(1)} %pad_maximum_fusion.1.u_ref), channel_id=1, source_target_pairs={{0,96},{1,33},{32,64},{33,1},{64,32},{65,97},{96,0},{97,65},{2,98}... | collective-permute-start | bytes 4325384 | tf_op jit(solution)/shard_map/ppermute | solution.py:31
  33.8 21.9 %collective-permute-start.10 = (bf16[4,352,128]{2,1,0:T(8,128)(2,1)S(1)}, bf16[4,352,128]{2,1,0:T(8,128)(2,1)S(1)}, u32[]{:S(2)}, u32[]{:S(2)}) collective-permute-start(bf16[4,352,128]{2,1,0:T(8,128)(2,1)S(1)} %get-tuple-element.36), channel_id=1, source_target_pairs={{0,96},{1,33},{32,64},{33,1},{64,32},{65,97},{96,0},{97,65},{2,98}... | collective-permute-start | bytes 1081352 | tf_op jit(solution)/shard_map/ppermute | solution.py:31
  35.3 21.7 %collective-permute-start.12 = (bf16[4,352,128]{2,1,0:T(8,128)(2,1)S(1)}, bf16[4,352,128]{2,1,0:T(8,128)(2,1)S(1)}, u32[]{:S(2)}, u32[]{:S(2)}) collective-permute-start(bf16[4,352,128]{2,1,0:T(8,128)(2,1)S(1)} %get-tuple-element.35), channel_id=1, source_target_pairs={{0,24},{1,9},{8,16},{9,1},{16,8},{17,25},{24,0},{25,17},{2,26},{3,... | collective-permute-start | bytes 1081352 | tf_op jit(solution)/shard_map/ppermute | solution.py:31
  55.8 13.2 %collective-permute-start.11 = (bf16[8,352,128]{2,1,0:T(8,128)(2,1)S(1)}, bf16[8,352,128]{2,1,0:T(8,128)(2,1)S(1)}, u32[]{:S(2)}, u32[]{:S(2)}) collective-permute-start(bf16[8,352,128]{2,1,0:T(8,128)(2,1)S(1)} %pad_maximum_fusion.5.refs_0_), channel_id=1, source_target_pairs={{0,24},{1,9},{8,16},{9,1},{16,8},{17,25},{24,0},{25,17},{2,26},{3,... | collective-permute-start | bytes 2162696 | tf_op jit(solution)/shard_map/ppermute | solution.py:31
  57.0 12.0 %collective-permute-start.13 = (bf16[8,352,128]{2,1,0:T(8,128)(2,1)S(1)}, bf16[8,352,128]{2,1,0:T(8,128)(2,1)S(1)}, u32[]{:S(2)}, u32[]{:S(2)}) collective-permute-start(bf16[8,352,128]{2,1,0:T(8,128)(2,1)S(1)} %pad_maximum_fusion.6.refs_1_), channel_id=1, source_target_pairs={{0,96},{1,33},{32,64},{33,1},{64,32},{65,97},{96,0},{97,65},{2,98}... | collective-permute-start | bytes 2162696 | tf_op jit(solution)/shard_map/ppermute | solution.py:31
  77.4 14.3 %collective-permute-start.17 = (bf16[576,2048]{1,0:T(8,128)(2,1)S(1)}, bf16[576,2048]{1,0:T(8,128)(2,1)S(1)}, u32[]{:S(2)}, u32[]{:S(2)}) collective-permute-start(bf16[576,2048]{1,0:T(8,128)(2,1)S(1)} %shard_map.67), channel_id=1, source_target_pairs={{0,1},{1,0},{2,3},{3,2},{4,5},{5,4},{6,7},{7,6},{8,9},{9,8},{10,11... | collective-permute-start | bytes 7077896 | tf_op jit(solution)/shard_map/ppermute | solution.py:232
  88.5 7.9 %collective-permute-start.20 = (bf16[256,2048]{1,0:T(8,128)(2,1)S(1)}, bf16[256,2048]{1,0:T(8,128)(2,1)S(1)}, u32[]{:S(2)}, u32[]{:S(2)}) collective-permute-start(bf16[256,2048]{1,0:T(8,128)(2,1)S(1)} %shard_map.70), channel_id=1, source_target_pairs={{0,1},{1,0},{2,3},{3,2},{4,5},{5,4},{6,7},{7,6},{8,9},{9,8},{10,11... | collective-permute-start | bytes 3145736 | tf_op jit(solution)/shard_map/ppermute | solution.py:232
  92.8 16.6 %collective-permute-start.18 = (bf16[288,2048]{1,0:T(8,128)(2,1)S(1)}, bf16[288,2048]{1,0:T(8,128)(2,1)S(1)}, u32[]{:S(2)}, u32[]{:S(2)}) collective-permute-start(bf16[288,2048]{1,0:T(8,128)(2,1)S(1)} %shard_map.68), channel_id=1, source_target_pairs={{0,2},{1,7},{2,0},{3,5},{4,6},{5,3},{6,4},{7,1},{8,10},{9,15},{10,... | collective-permute-start | bytes 3538952 | tf_op jit(solution)/shard_map/ppermute | solution.py:31
  96.4 4.5 %collective-permute-start.14 = (bf16[192,2048]{1,0:T(8,128)(2,1)S(1)}, bf16[192,2048]{1,0:T(8,128)(2,1)S(1)}, u32[]{:S(2)}, u32[]{:S(2)}) collective-permute-start(bf16[192,2048]{1,0:T(8,128)(2,1)S(1)} %shard_map.63), channel_id=1, source_target_pairs={{0,1},{1,0},{2,3},{3,2},{4,5},{5,4},{6,7},{7,6},{8,9},{9,8},{10,11... | collective-permute-start | bytes 2359304 | tf_op jit(solution)/shard_map/ppermute | solution.py:232
  97.1 17.9 %collective-permute-start.21 = (bf16[128,2048]{1,0:T(8,128)(2,1)S(1)}, bf16[128,2048]{1,0:T(8,128)(2,1)S(1)}, u32[]{:S(2)}, u32[]{:S(2)}) collective-permute-start(bf16[128,2048]{1,0:T(8,128)(2,1)S(1)} %shard_map.71), channel_id=1, source_target_pairs={{0,2},{1,7},{2,0},{3,5},{4,6},{5,3},{6,4},{7,1},{8,10},{9,15},{10,... | collective-permute-start | bytes 1572872 | tf_op jit(solution)/shard_map/ppermute | solution.py:31
  101.5 22.2 %collective-permute-start.15 = (bf16[96,2048]{1,0:T(8,128)(2,1)S(1)}, bf16[96,2048]{1,0:T(8,128)(2,1)S(1)}, u32[]{:S(2)}, u32[]{:S(2)}) collective-permute-start(bf16[96,2048]{1,0:T(8,128)(2,1)S(1)} %shard_map.65), channel_id=1, source_target_pairs={{0,2},{1,7},{2,0},{3,5},{4,6},{5,3},{6,4},{7,1},{8,10},{9,15},{10,... | collective-permute-start | bytes 1179656 | tf_op jit(solution)/shard_map/ppermute | solution.py:31
  110.5 18.5 %collective-permute-start.19 = (bf16[144,2048]{1,0:T(8,128)(2,1)S(1)}, bf16[144,2048]{1,0:T(8,128)(2,1)S(1)}, u32[]{:S(2)}, u32[]{:S(2)}) collective-permute-start(bf16[144,2048]{1,0:T(8,128)(2,1)S(1)} %get-tuple-element.32), channel_id=1, source_target_pairs={{0,6},{1,3},{2,4},{3,1},{4,2},{5,7},{6,0},{7,5},{8,14},{9,11},{10,... | collective-permute-start | bytes 1769480 | tf_op jit(solution)/shard_map/ppermute | solution.py:31
  115.6 12.6 %collective-permute-start.22 = (bf16[64,2048]{1,0:T(8,128)(2,1)S(1)}, bf16[64,2048]{1,0:T(8,128)(2,1)S(1)}, u32[]{:S(2)}, u32[]{:S(2)}) collective-permute-start(bf16[64,2048]{1,0:T(8,128)(2,1)S(1)} %get-tuple-element.34), channel_id=1, source_target_pairs={{0,6},{1,3},{2,4},{3,1},{4,2},{5,7},{6,0},{7,5},{8,14},{9,11},{10,... | collective-permute-start | bytes 786440 | tf_op jit(solution)/shard_map/ppermute | solution.py:31
  124.3 5.7 %collective-permute-start.16 = (bf16[48,2048]{1,0:T(8,128)(2,1)S(1)}, bf16[48,2048]{1,0:T(8,128)(2,1)S(1)}, u32[]{:S(2)}, u32[]{:S(2)}) collective-permute-start(bf16[48,2048]{1,0:T(8,128)(2,1)S(1)} %get-tuple-element.30), channel_id=1, source_target_pairs={{0,6},{1,3},{2,4},{3,1},{4,2},{5,7},{6,0},{7,5},{8,14},{9,11},{10,... | collective-permute-start | bytes 589832 | tf_op jit(solution)/shard_map/ppermute | solution.py:31
